TPU v7x, 32 devices: a whole 2x2x4 slice. The times are simulated.
32 devices in a mesh: ep: 8 (over z, core), tp: 4 (over y, x).
Axes of the slice: x: 2, y: 2, z: 4, core: 2. Of those that a mesh axis runs over, the one named last changes fastest.
Arguments:
- mixer_rows: bfloat16 [4096, 2048], P('ep', 'tp'), may hold values from -6 to 6
- expert_rows: bfloat16 [4096, 2048], P('ep', 'tp'), may hold values from -6 to 6
- mixer_gain: float32 [2048], replicated, may hold values from 0.1 to 1.9
- pool_scale: float32 [2048], P('tp'), may hold values from 0.1 to 1.9
- w_in: bfloat16 [2048, 2048], P(None, 'tp'), may hold values from -0.125 to 0.125
- w_mix_out: bfloat16 [2048, 2048], P(None, 'tp'), may hold values from -0.125 to 0.125
- expert_gain: float32 [2048], replicated, may hold values from 0.1 to 1.9
- expert_gate: bfloat16 [8, 2048, 2048], P('ep', None, 'tp'), may hold values from -0.125 to 0.125
- expert_up: bfloat16 [8, 2048, 2048], P('ep', None, 'tp'), may hold values from -0.125 to 0.125
- expert_down: bfloat16 [8, 2048, 2048], P('ep', None, 'tp'), may hold values from -0.125 to 0.125
- routes: int32 [4096, 2], P('ep'), may hold values from 0 to 7, all different within a row; in each aligned block of 512 rows (0 to 511, 512 to 1023, ...) at most 192 rows name the same one
- route_weight: float32 [4096, 2], P('ep'), may hold values from 0.1 to 1
Outputs:
- mixer_output: bfloat16 [4096, 2048], P('ep', 'tp')
- expert_output: bfloat16 [4096, 2048], P('ep', 'tp')
Inputs may be any that keep to these rules, and one draw needn't show every extreme that they name: `routes`: each row names 2 different experts. Among the rows of one device (aligned blocks of 512 rows) no expert is named more than 192 times, a bound that some block reaches.
All inputs are finite; a program needn't handle non-finite values.
Results may differ from a plain program's by a relative error of at most 0.0071.
Values may be sent and summed in bfloat16 or wider, within the bound.
No kernel may reach another device: no remote copies, remote signals or barrier semaphores. Data moves between devices by JAX's collectives and lax.ppermute only.
A program may use at most 64 MiB of HBM per device.

v0:
```python
import jax
import jax.numpy as jnp
from jax import lax
from jax.sharding import PartitionSpec as P

PW = 2048
TOP = 2


norm_eps = 1e-05
pool_windows = (2, 4, 8, 16)
rim_rows = 8
group_count = 4


def swapped(block, axis, bits):
    count = lax.axis_size(axis)
    return lax.ppermute(block, axis, [(i, i ^ bits) for i in range(count)])


class Plane:
    def __init__(self):
        self.past = []

    def exchange(self, to_second, to_first):
        if len(self.past) > 1:
            to_second, to_first, *_ = lax.optimization_barrier((to_second, to_first, *self.past[-2]))
        result = (swapped(to_second, "tp", 2), swapped(to_first, "tp", 1))
        self.past.append(result)
        return result

    def begin(self, block):
        if lax.axis_size("tp") != 4:
            return block
        second, first = self.exchange(block, block)
        return block, first, second

    def finish(self, begun):
        if lax.axis_size("tp") != 4:
            return lax.all_gather(begun, "tp", axis=1, tiled=True)
        block, first, second = begun
        half = block.shape[0] // 2
        top, bottom = self.exchange(first[:half], second[half:])
        return jnp.concatenate([block, first, second, jnp.concatenate([top, bottom], axis=0)], axis=1)


def arranged(weight, tp_index):
    count = lax.axis_size("tp")
    if count != 4:
        return weight
    width = weight.shape[0] // count
    return jnp.concatenate(
        [lax.dynamic_slice_in_dim(weight, (tp_index ^ j) * width, width, 0) for j in range(count)], axis=0
    )


def dot(a, b):
    return lax.dot_general(a, b, (((1,), (0,)), ((), ())), preferred_element_type=jnp.float32)


def layer_norm(row_block, gain_vec):
    values = row_block.astype(jnp.float32)
    center = values - jnp.mean(values, axis=-1, keepdims=True)
    spread = jnp.mean(center * center, axis=-1, keepdims=True)
    return (center * lax.rsqrt(spread + norm_eps) * gain_vec).astype(jnp.bfloat16)


def pooled_channels(inner, scale_local, ep_size, ep_index, tp_index):
    row_count, channels = inner.shape
    forward = [(i, i + 1) for i in range(ep_size - 1)]
    backward = [(target, source) for source, target in forward]
    low = lax.ppermute(inner[row_count - rim_rows :], "ep", forward)
    high = lax.ppermute(inner[:rim_rows], "ep", backward)
    extended = jnp.concatenate([low, inner, high], axis=0)
    group = tp_index * channels // (PW // len(pool_windows))
    window = jnp.left_shift(jnp.int32(pool_windows[0]), group)
    half_span = window // 2
    seq_len = row_count * ep_size
    row = jnp.arange(row_count, dtype=jnp.int32)[:, None]
    column = jnp.arange(row_count + 2 * rim_rows, dtype=jnp.int32)[None, :] - rim_rows
    band = ((column >= row - half_span) & (column < row + half_span)).astype(jnp.bfloat16)
    position = ep_index * row_count + row
    lower_end = jnp.clip(position - half_span, 0, seq_len)
    upper_end = jnp.clip(position - half_span + window, 0, seq_len)
    counts = (upper_end - lower_end).astype(jnp.float32)
    values = inner.astype(jnp.float32)
    return ((dot(band, extended) / counts - values) * scale_local[None, :]).astype(jnp.bfloat16)


def on_device(
    mixer_rows,
    expert_rows,
    mixer_gain,
    pool_scale,
    w_in,
    w_mix_out,
    expert_gain,
    expert_gate,
    expert_up,
    expert_down,
    routes,
    route_weight,
):
    ep_size = lax.axis_size("ep")
    ep_index = lax.axis_index("ep")
    tp_index = lax.axis_index("tp")
    row_count = routes.shape[0]
    capacity = (3 * TOP * row_count + 2 * ep_size - 1) // (2 * ep_size)
    blocks = max(1, ep_size // group_count)
    groups = ep_size // blocks
    slot = jnp.arange(blocks * capacity, dtype=jnp.int32)
    plane = Plane()

    mix = plane.begin(mixer_rows)

    experts = jnp.arange(ep_size, dtype=jnp.int32)
    chosen = routes[:, :, None] == experts[None, None, :]
    named = (chosen[:, 0] | chosen[:, 1]).astype(jnp.bfloat16)
    row = jnp.arange(row_count, dtype=jnp.int32)
    earlier = (row[None, :] < row[:, None]).astype(jnp.bfloat16)
    ahead = dot(earlier, named)
    ranking = jnp.sum(jnp.where(chosen, ahead[:, None, :], 0.0), axis=2).astype(jnp.int32)
    place = (routes ^ ep_index) * capacity + ranking
    place_rows = place.T

    def crossed(rows, group):
        pieces = []
        for b in range(blocks):
            shift = group * blocks + b
            piece = rows[b * capacity : (b + 1) * capacity]
            pieces.append(piece if shift == 0 else swapped(piece, "ep", shift))
        return jnp.concatenate(pieces, axis=0)

    order = [0] + list(range(groups - 1, 0, -1))
    arrived = {}
    after = place_rows
    for group in order:
        slots = slot + group * blocks * capacity
        picks = (slots[:, None] == after[0][None, :]) | (slots[:, None] == after[1][None, :])
        outgoing = dot(picks.astype(jnp.bfloat16), expert_rows).astype(jnp.bfloat16)
        after, outgoing = lax.optimization_barrier((place_rows, outgoing))
        arrived[group] = crossed(outgoing, group)

    gain = arranged(expert_gain, tp_index)
    gate_up = arranged(jnp.concatenate([expert_gate[0], expert_up[0]], axis=1), tp_index)
    down_weight = arranged(expert_down[0], tp_index)

    def hidden_of(slots):
        both = dot(layer_norm(slots, gain), gate_up)
        units = both.shape[1] // 2
        return (jax.nn.silu(both[:, :units]) * both[:, units:]).astype(jnp.bfloat16)

    returned = {}

    def send_back(group, begun):
        full = plane.finish(begun)
        value = dot(full, down_weight).astype(jnp.bfloat16)
        returned[group] = crossed(value, group)

    hidden = {}
    rows = plane.begin(arrived[0])
    full_mix = plane.finish(mix)
    hidden[0] = hidden_of(plane.finish(rows))
    mix_weight = arranged(w_in, tp_index)
    mix_normed = layer_norm(full_mix, arranged(mixer_gain, tp_index))
    inner = dot(mix_normed, mix_weight).astype(jnp.bfloat16)
    pooled = pooled_channels(inner, pool_scale, ep_size, ep_index, tp_index)
    waiting = plane.begin(pooled)
    finish_mix = True
    behind = None
    for group in order[1:]:
        rows = plane.begin(arrived[group])
        if finish_mix:
            full_pooled = plane.finish(waiting)
            out_weight = arranged(w_mix_out, tp_index)
            mixer_output = dot(full_pooled, out_weight).astype(jnp.bfloat16)
            finish_mix = False
        else:
            hidden[behind[0]] = hidden_of(plane.finish(behind[1]))
        behind = (group, rows)
    queue = order[1:] + order[:1]
    begun = plane.begin(hidden[queue[0]])
    hidden[behind[0]] = hidden_of(plane.finish(behind[1]))
    for index, group in enumerate(queue):
        if index + 1 < len(queue):
            following = plane.begin(hidden[queue[index + 1]])
        send_back(group, begun)
        begun = following

    total = jnp.zeros((row_count, expert_down.shape[2]), jnp.float32)
    for group in queue:
        slots = slot + group * blocks * capacity
        for k in range(TOP):
            picks = (place[:, k][:, None] == slots[None, :]).astype(jnp.bfloat16)
            total = total + dot(picks, returned[group]) * route_weight[:, k][:, None]
    return (mixer_output, total.astype(jnp.bfloat16))


def solution(mesh):
    return mapped(mesh)


def mapped(mesh):
    return jax.shard_map(
        on_device,
        mesh=mesh,
        in_specs=(
            P("ep", "tp"),
            P("ep", "tp"),
            P(),
            P("tp"),
            P(None, "tp"),
            P(None, "tp"),
            P(),
            P("ep", None, "tp"),
            P("ep", None, "tp"),
            P("ep", None, "tp"),
            P("ep", None),
            P("ep", None),
        ),
        out_specs=(P("ep", "tp"), P("ep", "tp")),
        check_vma=False,
    )
```

profile of v0, /device:TPU:0, one launch (start us, length us, event | category | flops | bytes accessed | tf_op | source)
XLA Modules:
  0.0 225.1 jit_solution(10726980605473655933)
XLA Ops:
  0.6 3.0 %collective-permute-start = (bf16[512,512]{1,0:T(8,128)(2,1)}, bf16[512,512]{1,0:T(8,128)(2,1)S(1)}, u32[]{:S(2)}, u32[]{:S(2)}) collective-permute-start(bf16[512,512]{1,0:T(8,128)(2,1)} %param.12), channel_id=1, source_target_pairs={{0,1},{1,0},{2,3},{3,2},{4,5},{5,4},{6,7},{7,6},{8,9},{9,8},{10,11... | collective-permute-start | bytes 1572872 | tf_op jit(solution)/shard_map/ppermute | solution.py:18
  3.7 1.5 collective-permute-start.1
  8.7 1.2 convolution_convert_fusion.2
  9.9 1.2 convolution_convert_fusion.1
  12.3 1.6 collective-permute-start.21
  14.1 1.4 constant_dynamic-slice_fusion.3
  16.5 1.4 constant_dynamic-slice_fusion.7
  19.5 3.0 %dynamic-slice_bitcast_fusion.3 = (bf16[512,512]{1,0:T(8,128)(2,1)}, bf16[512,512]{1,0:T(8,128)(2,1)}, bf16[512,512]{1,0:T(8,128)(2,1)}, bf16[512,512]{1,0:T(8,128)(2,1)}) fusion(bf16[1,2048,512]{2,1,0:T(8,128)(2,1)} %param.21, s32[]{:T(128)S(6)} %select_n.21, s32[]{:T(128)S(6)} %select_n.22, s32[]{:T(128)S(6)} %select_n.25, s32[]{:T(128)S(6)} %select_n.24), kind=kLoop, calls=%fused_computation.212 | loop fusion | bytes 4194320 | tf_op jit(solution)/shard_map/dynamic_slice | solution.py:53
  22.7 2.1 fusion.153
  24.8 2.7 %collective-permute-start.23 = (bf16[192,512]{1,0:T(8,128)(2,1)S(1)}, bf16[192,512]{1,0:T(8,128)(2,1)S(1)}, u32[]{:S(2)}, u32[]{:S(2)}) collective-permute-start(bf16[192,512]{1,0:T(8,128)(2,1)S(1)} %copy-done.23), channel_id=1, source_target_pairs={{0,16},{4,20},{8,24},{12,28},{16,0},{20,4},{24,8},{28,12},{1,17},{... | collective-permute-start | bytes 589832 | tf_op jit(solution)/shard_map/ppermute | solution.py:18
  27.6 1.4 collective-permute-start.10
  29.9 12.1 %collective-permute-done.23 = bf16[192,512]{1,0:T(8,128)(2,1)S(1)} collective-permute-done((bf16[192,512]{1,0:T(8,128)(2,1)S(1)}, bf16[192,512]{1,0:T(8,128)(2,1)S(1)}, u32[]{:S(2)}, u32[]{:S(2)}) %collective-permute-start.23) | collective-permute-done | bytes 196640 | tf_op jit(solution)/shard_map/ppermute | solution.py:18
  43.0 2.1 collective-permute-start.11
  46.2 1.6 collective-permute-start.3
  47.7 10.4 %collective-permute-done.24 = bf16[192,512]{1,0:T(8,128)(2,1)S(1)} collective-permute-done((bf16[192,512]{1,0:T(8,128)(2,1)S(1)}, bf16[192,512]{1,0:T(8,128)(2,1)S(1)}, u32[]{:S(2)}, u32[]{:S(2)}) %collective-permute-start.24) | collective-permute-done | bytes 196640 | tf_op jit(solution)/shard_map/ppermute | solution.py:18
  60.3 1.6 collective-permute-start.15
  61.9 5.5 %collective-permute-done.2 = bf16[256,512]{1,0:T(8,128)(2,1)S(1)} collective-permute-done((bf16[256,512]{1,0:T(8,128)(2,1)S(1)}, bf16[256,512]{1,0:T(8,128)(2,1)S(1)}, u32[]{:S(2)}, u32[]{:S(2)}) %collective-permute-start.2) | collective-permute-done | bytes 262176 | tf_op jit(solution)/shard_map/ppermute | solution.py:18
  67.4 5.0 %convert_reduce_fusion = (f32[512]{0:T(512)S(1)}, bf16[512,2048]{1,0:T(8,128)(2,1)S(1)}) fusion(bf16[256,512]{1,0:T(8,128)(2,1)S(1)} %collective-permute-done.3, bf16[256,512]{1,0:T(8,128)(2,1)S(1)} %collective-permute-done.2, bf16[512,512]{1,0:T(8,128)(2,1)} %collective-permute-done.1, bf16[512,512]{1,0:T(8,128)(2,1)S(1)} %collective-permute-done, ...), kind=kLoop, calls=%fused_computation.9 | loop fusion | flops 12582400 | bytes 4196352 | tf_op jit(solution)/shard_map/reduce_sum | solution.py:63
  73.9 1.3 fusion.135
  75.2 1.3 collective-permute-start.5
  76.5 3.2 %collective-permute-start.4 = (bf16[8,512]{1,0:T(8,128)(2,1)S(1)}, bf16[8,512]{1,0:T(8,128)(2,1)S(1)}, u32[]{:S(2)}, u32[]{:S(2)}) collective-permute-start(bf16[8,512]{1,0:T(8,128)(2,1)S(1)} %get-tuple-element.114), channel_id=1, source_target_pairs={{0,4},{4,8},{8,12},{12,16},{16,20},{20,24},{24,28},{1,5},{5,9},{9,... | collective-permute-start | bytes 24584 | tf_op jit(solution)/shard_map/ppermute | solution.py:72
  82.1 1.6 collective-permute-start.18
  83.7 1.5 collective-permute-start.17
  85.7 14.4 %collective-permute-done.18 = bf16[384,512]{1,0:T(8,128)(2,1)S(1)} collective-permute-done((bf16[384,512]{1,0:T(8,128)(2,1)S(1)}, bf16[384,512]{1,0:T(8,128)(2,1)S(1)}, u32[]{:S(2)}, u32[]{:S(2)}) %collective-permute-start.18) | collective-permute-done | bytes 393248 | tf_op jit(solution)/shard_map/ppermute | solution.py:18
  100.7 2.3 %collective-permute-start.26 = (bf16[384,512]{1,0:T(8,128)(2,1)S(1)}, bf16[384,512]{1,0:T(8,128)(2,1)S(1)}, u32[]{:S(2)}, u32[]{:S(2)}) collective-permute-start(bf16[384,512]{1,0:T(8,128)(2,1)S(1)} %constant_dynamic-update-slice_fusion.4), channel_id=1, source_target_pairs={{0,1},{1,0},{2,3},{3,2},{4,5},{5,4},{6,7},{7,6},{8,9},{9,8},{10,11... | collective-permute-start | bytes 1179656 | tf_op jit(solution)/shard_map/ppermute | solution.py:18
  103.2 1.6 collective-permute-start.8
  104.8 1.9 fusion.60
  107.0 2.5 %collective-permute-done.25 = bf16[384,512]{1,0:T(8,128)(2,1)S(1)} collective-permute-done((bf16[384,512]{1,0:T(8,128)(2,1)S(1)}, bf16[384,512]{1,0:T(8,128)(2,1)S(1)}, u32[]{:S(2)}, u32[]{:S(2)}) %collective-permute-start.25) | collective-permute-done | bytes 393248 | tf_op jit(solution)/shard_map/ppermute | solution.py:18
  109.6 2.5 %collective-permute-start.28 = (bf16[384,512]{1,0:T(8,128)(2,1)S(1)}, bf16[384,512]{1,0:T(8,128)(2,1)S(1)}, u32[]{:S(2)}, u32[]{:S(2)}) collective-permute-start(bf16[384,512]{1,0:T(8,128)(2,1)S(1)} %constant_dynamic-update-slice_fusion.2), channel_id=1, source_target_pairs={{0,1},{1,0},{2,3},{3,2},{4,5},{5,4},{6,7},{7,6},{8,9},{9,8},{10,11... | collective-permute-start | bytes 1179656 | tf_op jit(solution)/shard_map/ppermute | solution.py:18
  112.1 1.5 collective-permute-start.27
  113.6 1.6 collective-permute-done.9
  115.2 1.5 collective-permute-start.19
  116.7 2.5 %collective-permute-start.20 = (bf16[192,512]{1,0:T(8,128)(2,1)S(1)}, bf16[192,512]{1,0:T(8,128)(2,1)S(1)}, u32[]{:S(2)}, u32[]{:S(2)}) collective-permute-start(bf16[192,512]{1,0:T(8,128)(2,1)S(1)} %slice.266), channel_id=1, source_target_pairs={{0,1},{1,0},{2,3},{3,2},{4,5},{5,4},{6,7},{7,6},{8,9},{9,8},{10,11... | collective-permute-start | bytes 589832 | tf_op jit(solution)/shard_map/ppermute | solution.py:18
  119.2 2.1 fusion.130
  121.3 7.0 %collective-permute-done.19 = bf16[192,512]{1,0:T(8,128)(2,1)S(1)} collective-permute-done((bf16[192,512]{1,0:T(8,128)(2,1)S(1)}, bf16[192,512]{1,0:T(8,128)(2,1)S(1)}, u32[]{:S(2)}, u32[]{:S(2)}) %collective-permute-start.19) | collective-permute-done | bytes 196640 | tf_op jit(solution)/shard_map/ppermute | solution.py:18
  128.3 1.2 collective-permute-start.31
  129.5 2.4 %collective-permute-start.32 = (bf16[192,512]{1,0:T(8,128)(2,1)S(1)}, bf16[192,512]{1,0:T(8,128)(2,1)S(1)}, u32[]{:S(2)}, u32[]{:S(2)}) collective-permute-start(bf16[192,512]{1,0:T(8,128)(2,1)S(1)} %slice.274), channel_id=1, source_target_pairs={{0,1},{1,0},{2,3},{3,2},{4,5},{5,4},{6,7},{7,6},{8,9},{9,8},{10,11... | collective-permute-start | bytes 589832 | tf_op jit(solution)/shard_map/ppermute | solution.py:18
  132.7 1.9 fusion.54
  135.8 2.3 %collective-permute-start.34 = (bf16[192,512]{1,0:T(8,128)(2,1)S(1)}, bf16[192,512]{1,0:T(8,128)(2,1)S(1)}, u32[]{:S(2)}, u32[]{:S(2)}) collective-permute-start(bf16[192,512]{1,0:T(8,128)(2,1)S(1)} %slice.272), channel_id=1, source_target_pairs={{0,1},{1,0},{2,3},{3,2},{4,5},{5,4},{6,7},{7,6},{8,9},{9,8},{10,11... | collective-permute-start | bytes 589832 | tf_op jit(solution)/shard_map/ppermute | solution.py:18
  138.1 1.0 collective-permute-start.33
  140.0 1.9 fusion.56
  142.1 8.6 %collective-permute-done.34 = bf16[192,512]{1,0:T(8,128)(2,1)S(1)} collective-permute-done((bf16[192,512]{1,0:T(8,128)(2,1)S(1)}, bf16[192,512]{1,0:T(8,128)(2,1)S(1)}, u32[]{:S(2)}, u32[]{:S(2)}) %collective-permute-start.34) | collective-permute-done | bytes 196640 | tf_op jit(solution)/shard_map/ppermute | solution.py:18
  151.6 1.6 collective-permute-start.35
  153.2 2.1 fusion.58
  155.3 1.5 collective-permute-start.40
  156.9 1.1 collective-permute-start.39
  157.9 1.5 collective-permute-done.35
  159.5 1.5 collective-permute-done.36
  162.0 4.4 %collective-permute-start.37 = (bf16[192,512]{1,0:T(8,128)(2,1)S(1)}, bf16[192,512]{1,0:T(8,128)(2,1)S(1)}, u32[]{:S(2)}, u32[]{:S(2)}) collective-permute-start(bf16[192,512]{1,0:T(8,128)(2,1)S(1)} %get-tuple-element.117), channel_id=1, source_target_pairs={{0,24},{4,28},{8,16},{12,20},{16,8},{20,12},{24,0},{28,4},{1,25},{... | collective-permute-start | bytes 589832 | tf_op jit(solution)/shard_map/ppermute | solution.py:18
  166.7 1.1 collective-permute-done.40
  167.7 1.2 collective-permute-done.39
  171.4 1.9 collective-permute-start.42
  173.3 1.1 collective-permute-done.38
  174.4 9.5 %collective-permute-done.41 = bf16[192,512]{1,0:T(8,128)(2,1)S(1)} collective-permute-done((bf16[192,512]{1,0:T(8,128)(2,1)S(1)}, bf16[192,512]{1,0:T(8,128)(2,1)S(1)}, u32[]{:S(2)}, u32[]{:S(2)}) %collective-permute-start.41) | collective-permute-done | bytes 196640 | tf_op jit(solution)/shard_map/ppermute | solution.py:18
  185.1 5.5 %collective-permute-start.43 = (bf16[192,512]{1,0:T(8,128)(2,1)S(1)}, bf16[192,512]{1,0:T(8,128)(2,1)S(1)}, u32[]{:S(2)}, u32[]{:S(2)}) collective-permute-start(bf16[192,512]{1,0:T(8,128)(2,1)S(1)} %get-tuple-element.119), channel_id=1, source_target_pairs={{0,16},{4,20},{8,24},{12,28},{16,0},{20,4},{24,8},{28,12},{1,17},{... | collective-permute-start | bytes 589832 | tf_op jit(solution)/shard_map/ppermute | solution.py:18
  191.9 1.8 collective-permute-start.48
  193.7 10.1 %collective-permute-done.43 = bf16[192,512]{1,0:T(8,128)(2,1)S(1)} collective-permute-done((bf16[192,512]{1,0:T(8,128)(2,1)S(1)}, bf16[192,512]{1,0:T(8,128)(2,1)S(1)}, u32[]{:S(2)}, u32[]{:S(2)}) %collective-permute-start.43) | collective-permute-done | bytes 196640 | tf_op jit(solution)/shard_map/ppermute | solution.py:18
  203.8 1.1 collective-permute-start.47
  204.9 1.9 collective-permute-done.44
  207.2 2.2 collective-permute-done.47
  211.2 1.3 collective-permute-start.54
  212.9 4.9 %collective-permute-done.49 = bf16[192,512]{1,0:T(8,128)(2,1)S(1)} collective-permute-done((bf16[192,512]{1,0:T(8,128)(2,1)S(1)}, bf16[192,512]{1,0:T(8,128)(2,1)S(1)}, u32[]{:S(2)}, u32[]{:S(2)}) %collective-permute-start.49) | collective-permute-done | bytes 196640 | tf_op jit(solution)/shard_map/ppermute | solution.py:18
  218.5 1.0 collective-permute-done.53
  223.4 1.7 fusion.126
  (220 shorter events, 35.7 us)
Async XLA Ops:
  0.6 42.0 %collective-permute-start = (bf16[512,512]{1,0:T(8,128)(2,1)}, bf16[512,512]{1,0:T(8,128)(2,1)S(1)}, u32[]{:S(2)}, u32[]{:S(2)}) collective-permute-start(bf16[512,512]{1,0:T(8,128)(2,1)} %param.12), channel_id=1, source_target_pairs={{0,1},{1,0},{2,3},{3,2},{4,5},{5,4},{6,7},{7,6},{8,9},{9,8},{10,11... | collective-permute-start | bytes 1572872 | tf_op jit(solution)/shard_map/ppermute | solution.py:18
  3.7 39.3 %collective-permute-start.1 = (bf16[512,512]{1,0:T(8,128)(2,1)}, bf16[512,512]{1,0:T(8,128)(2,1)}, u32[]{:S(2)}, u32[]{:S(2)}) collective-permute-start(bf16[512,512]{1,0:T(8,128)(2,1)} %param.12), channel_id=1, source_target_pairs={{0,2},{1,3},{2,0},{3,1},{4,6},{5,7},{6,4},{7,5},{8,10},{9,11},{10,... | collective-permute-start | bytes 1572872 | tf_op jit(solution)/shard_map/ppermute | solution.py:18
  8.7 16.2 %collective-permute-start.12 = (bf16[192,512]{1,0:T(8,128)(2,1)}, bf16[192,512]{1,0:T(8,128)(2,1)S(1)}, u32[]{:S(2)}, u32[]{:S(2)}) collective-permute-start(bf16[192,512]{1,0:T(8,128)(2,1)} %get-tuple-element.131), channel_id=1, source_target_pairs={{0,4},{4,0},{8,12},{12,8},{16,20},{20,16},{24,28},{28,24},{1,5},{5... | collective-permute-start | bytes 589832 | tf_op jit(solution)/shard_map/ppermute | solution.py:18
  12.3 15.3 %collective-permute-start.21 = (bf16[192,512]{1,0:T(8,128)(2,1)}, bf16[192,512]{1,0:T(8,128)(2,1)}, u32[]{:S(2)}, u32[]{:S(2)}) collective-permute-start(bf16[192,512]{1,0:T(8,128)(2,1)} %get-tuple-element.129), channel_id=1, source_target_pairs={{0,8},{4,12},{8,0},{12,4},{16,24},{20,28},{24,16},{28,20},{1,9},{5... | collective-permute-start | bytes 589832 | tf_op jit(solution)/shard_map/ppermute | solution.py:18
  13.8 32.3 %collective-permute-start.22 = (bf16[192,512]{1,0:T(8,128)(2,1)}, bf16[192,512]{1,0:T(8,128)(2,1)}, u32[]{:S(2)}, u32[]{:S(2)}) collective-permute-start(bf16[192,512]{1,0:T(8,128)(2,1)} %get-tuple-element.128), channel_id=1, source_target_pairs={{0,12},{4,8},{8,4},{12,0},{16,28},{20,24},{24,20},{28,16},{1,13},{... | collective-permute-start | bytes 589832 | tf_op jit(solution)/shard_map/ppermute | solution.py:18
  22.6 19.4 %copy-start.21 = (bf16[192,512]{1,0:T(8,128)(2,1)S(1)}, bf16[192,512]{1,0:T(8,128)(2,1)}, u32[]{:S(2)}) copy-start(bf16[192,512]{1,0:T(8,128)(2,1)} %get-tuple-element.126) | copy-start | bytes 589828
  24.7 18.3 %copy-start.20 = (bf16[192,512]{1,0:T(8,128)(2,1)S(1)}, bf16[192,512]{1,0:T(8,128)(2,1)}, u32[]{:S(2)}) copy-start(bf16[192,512]{1,0:T(8,128)(2,1)} %get-tuple-element.124) | copy-start | bytes 589828
  24.8 17.2 %collective-permute-start.23 = (bf16[192,512]{1,0:T(8,128)(2,1)S(1)}, bf16[192,512]{1,0:T(8,128)(2,1)S(1)}, u32[]{:S(2)}, u32[]{:S(2)}) collective-permute-start(bf16[192,512]{1,0:T(8,128)(2,1)S(1)} %copy-done.23), channel_id=1, source_target_pairs={{0,16},{4,20},{8,24},{12,28},{16,0},{20,4},{24,8},{28,12},{1,17},{... | collective-permute-start | bytes 589832 | tf_op jit(solution)/shard_map/ppermute | solution.py:18
  27.5 39.8 %copy-start.5 = (bf16[512,512]{1,0:T(8,128)(2,1)S(1)}, bf16[512,512]{1,0:T(8,128)(2,1)}, u32[]{:S(2)}) copy-start(bf16[512,512]{1,0:T(8,128)(2,1)} %param.12) | copy-start | bytes 1572868
  27.6 14.5 %collective-permute-start.10 = (bf16[192,512]{1,0:T(8,128)(2,1)S(1)}, bf16[192,512]{1,0:T(8,128)(2,1)S(1)}, u32[]{:S(2)}, u32[]{:S(2)}) collective-permute-start(bf16[192,512]{1,0:T(8,128)(2,1)S(1)} %copy-done.22), channel_id=1, source_target_pairs={{0,24},{4,28},{8,16},{12,20},{16,8},{20,12},{24,0},{28,4},{1,25},{... | collective-permute-start | bytes 589832 | tf_op jit(solution)/shard_map/ppermute | solution.py:18
  42.0 16.2 %collective-permute-start.24 = (bf16[192,512]{1,0:T(8,128)(2,1)S(1)}, bf16[192,512]{1,0:T(8,128)(2,1)S(1)}, u32[]{:S(2)}, u32[]{:S(2)}) collective-permute-start(bf16[192,512]{1,0:T(8,128)(2,1)S(1)} %copy-done.21), channel_id=1, source_target_pairs={{0,20},{4,16},{8,28},{12,24},{16,4},{20,0},{24,12},{28,8},{1,21},{... | collective-permute-start | bytes 589832 | tf_op jit(solution)/shard_map/ppermute | solution.py:18
  42.0 17.6 %collective-permute-start.13 = (bf16[384,512]{1,0:T(8,128)(2,1)S(1)}, bf16[384,512]{1,0:T(8,128)(2,1)S(1)}, u32[]{:S(2)}, u32[]{:S(2)}) collective-permute-start(bf16[384,512]{1,0:T(8,128)(2,1)S(1)} %pad_maximum_fusion.2), channel_id=1, source_target_pairs={{0,1},{1,0},{2,3},{3,2},{4,5},{5,4},{6,7},{7,6},{8,9},{9,8},{10,11... | collective-permute-start | bytes 1179656 | tf_op jit(solution)/shard_map/ppermute | solution.py:18
  42.7 17.1 %collective-permute-start.14 = (bf16[384,512]{1,0:T(8,128)(2,1)S(1)}, bf16[384,512]{1,0:T(8,128)(2,1)S(1)}, u32[]{:S(2)}, u32[]{:S(2)}) collective-permute-start(bf16[384,512]{1,0:T(8,128)(2,1)S(1)} %pad_maximum_fusion.2), channel_id=1, source_target_pairs={{0,2},{1,3},{2,0},{3,1},{4,6},{5,7},{6,4},{7,5},{8,10},{9,11},{10,... | collective-permute-start | bytes 1179656 | tf_op jit(solution)/shard_map/ppermute | solution.py:18
  43.0 16.6 %collective-permute-start.11 = (bf16[192,512]{1,0:T(8,128)(2,1)S(1)}, bf16[192,512]{1,0:T(8,128)(2,1)S(1)}, u32[]{:S(2)}, u32[]{:S(2)}) collective-permute-start(bf16[192,512]{1,0:T(8,128)(2,1)S(1)} %copy-done.20), channel_id=1, source_target_pairs={{0,28},{4,24},{8,20},{12,16},{16,12},{20,8},{24,4},{28,0},{1,29},{... | collective-permute-start | bytes 589832 | tf_op jit(solution)/shard_map/ppermute | solution.py:18
  46.2 15.7 %collective-permute-start.3 = (bf16[256,512]{1,0:T(8,128)(2,1)S(1)}, bf16[256,512]{1,0:T(8,128)(2,1)S(1)}, u32[]{:S(2)}, u32[]{:S(2)}) collective-permute-start(bf16[256,512]{1,0:T(8,128)(2,1)S(1)} %slice.253), channel_id=1, source_target_pairs={{0,1},{1,0},{2,3},{3,2},{4,5},{5,4},{6,7},{7,6},{8,9},{9,8},{10,11... | collective-permute-start | bytes 786440 | tf_op jit(solution)/shard_map/ppermute | solution.py:18
  58.2 9.2 %collective-permute-start.2 = (bf16[256,512]{1,0:T(8,128)(2,1)S(1)}, bf16[256,512]{1,0:T(8,128)(2,1)S(1)}, u32[]{:S(2)}, u32[]{:S(2)}) collective-permute-start(bf16[256,512]{1,0:T(8,128)(2,1)S(1)} %slice.252), channel_id=1, source_target_pairs={{0,2},{1,3},{2,0},{3,1},{4,6},{5,7},{6,4},{7,5},{8,10},{9,11},{10,... | collective-permute-start | bytes 786440 | tf_op jit(solution)/shard_map/ppermute | solution.py:18
  59.8 20.0 %collective-permute-start.16 = (bf16[192,512]{1,0:T(8,128)(2,1)S(1)}, bf16[192,512]{1,0:T(8,128)(2,1)S(1)}, u32[]{:S(2)}, u32[]{:S(2)}) collective-permute-start(bf16[192,512]{1,0:T(8,128)(2,1)S(1)} %slice.264), channel_id=1, source_target_pairs={{0,1},{1,0},{2,3},{3,2},{4,5},{5,4},{6,7},{7,6},{8,9},{9,8},{10,11... | collective-permute-start | bytes 589832 | tf_op jit(solution)/shard_map/ppermute | solution.py:18
  60.3 19.4 %collective-permute-start.15 = (bf16[192,512]{1,0:T(8,128)(2,1)S(1)}, bf16[192,512]{1,0:T(8,128)(2,1)S(1)}, u32[]{:S(2)}, u32[]{:S(2)}) collective-permute-start(bf16[192,512]{1,0:T(8,128)(2,1)S(1)} %slice.263), channel_id=1, source_target_pairs={{0,2},{1,3},{2,0},{3,1},{4,6},{5,7},{6,4},{7,5},{8,10},{9,11},{10,... | collective-permute-start | bytes 589832 | tf_op jit(solution)/shard_map/ppermute | solution.py:18
  75.2 4.8 %collective-permute-start.5 = (bf16[8,512]{1,0:T(8,128)(2,1)S(1)}, bf16[8,512]{1,0:T(8,128)(2,1)S(1)}, u32[]{:S(2)}, u32[]{:S(2)}) collective-permute-start(bf16[8,512]{1,0:T(8,128)(2,1)S(1)} %get-tuple-element.115), channel_id=1, source_target_pairs={{4,0},{8,4},{12,8},{16,12},{20,16},{24,20},{28,24},{5,1},{9,5},{13... | collective-permute-start | bytes 24584 | tf_op jit(solution)/shard_map/ppermute | solution.py:73
  76.5 3.8 %collective-permute-start.4 = (bf16[8,512]{1,0:T(8,128)(2,1)S(1)}, bf16[8,512]{1,0:T(8,128)(2,1)S(1)}, u32[]{:S(2)}, u32[]{:S(2)}) collective-permute-start(bf16[8,512]{1,0:T(8,128)(2,1)S(1)} %get-tuple-element.114), channel_id=1, source_target_pairs={{0,4},{4,8},{8,12},{12,16},{16,20},{20,24},{24,28},{1,5},{5,9},{9,... | collective-permute-start | bytes 24584 | tf_op jit(solution)/shard_map/ppermute | solution.py:72
  81.0 22.0 %collective-permute-start.6 = (bf16[512,512]{1,0:T(8,128)(2,1)S(1)}, bf16[512,512]{1,0:T(8,128)(2,1)S(1)}, u32[]{:S(2)}, u32[]{:S(2)}) collective-permute-start(bf16[512,512]{1,0:T(8,128)(2,1)S(1)} %fusion.127), channel_id=1, source_target_pairs={{0,1},{1,0},{2,3},{3,2},{4,5},{5,4},{6,7},{7,6},{8,9},{9,8},{10,11... | collective-permute-start | bytes 1572872 | tf_op jit(solution)/shard_map/ppermute | solution.py:18
  81.6 21.4 %collective-permute-start.7 = (bf16[512,512]{1,0:T(8,128)(2,1)S(1)}, bf16[512,512]{1,0:T(8,128)(2,1)S(1)}, u32[]{:S(2)}, u32[]{:S(2)}) collective-permute-start(bf16[512,512]{1,0:T(8,128)(2,1)S(1)} %fusion.127), channel_id=1, source_target_pairs={{0,2},{1,3},{2,0},{3,1},{4,6},{5,7},{6,4},{7,5},{8,10},{9,11},{10,... | collective-permute-start | bytes 1572872 | tf_op jit(solution)/shard_map/ppermute | solution.py:18
  82.1 18.0 %collective-permute-start.18 = (bf16[384,512]{1,0:T(8,128)(2,1)S(1)}, bf16[384,512]{1,0:T(8,128)(2,1)S(1)}, u32[]{:S(2)}, u32[]{:S(2)}) collective-permute-start(bf16[384,512]{1,0:T(8,128)(2,1)S(1)} %constant_dynamic-update-slice_fusion), channel_id=1, source_target_pairs={{0,2},{1,3},{2,0},{3,1},{4,6},{5,7},{6,4},{7,5},{8,10},{9,11},{10,... | collective-permute-start | bytes 1179656 | tf_op jit(solution)/shard_map/ppermute | solution.py:18
  83.7 16.5 %collective-permute-start.17 = (bf16[384,512]{1,0:T(8,128)(2,1)S(1)}, bf16[384,512]{1,0:T(8,128)(2,1)S(1)}, u32[]{:S(2)}, u32[]{:S(2)}) collective-permute-start(bf16[384,512]{1,0:T(8,128)(2,1)S(1)} %constant_dynamic-update-slice_fusion), channel_id=1, source_target_pairs={{0,1},{1,0},{2,3},{3,2},{4,5},{5,4},{6,7},{7,6},{8,9},{9,8},{10,11... | collective-permute-start | bytes 1179656 | tf_op jit(solution)/shard_map/ppermute | solution.py:18
  100.2 9.3 %collective-permute-start.25 = (bf16[384,512]{1,0:T(8,128)(2,1)S(1)}, bf16[384,512]{1,0:T(8,128)(2,1)S(1)}, u32[]{:S(2)}, u32[]{:S(2)}) collective-permute-start(bf16[384,512]{1,0:T(8,128)(2,1)S(1)} %constant_dynamic-update-slice_fusion.4), channel_id=1, source_target_pairs={{0,2},{1,3},{2,0},{3,1},{4,6},{5,7},{6,4},{7,5},{8,10},{9,11},{10,... | collective-permute-start | bytes 1179656 | tf_op jit(solution)/shard_map/ppermute | solution.py:18
  100.7 8.9 %collective-permute-start.26 = (bf16[384,512]{1,0:T(8,128)(2,1)S(1)}, bf16[384,512]{1,0:T(8,128)(2,1)S(1)}, u32[]{:S(2)}, u32[]{:S(2)}) collective-permute-start(bf16[384,512]{1,0:T(8,128)(2,1)S(1)} %constant_dynamic-update-slice_fusion.4), channel_id=1, source_target_pairs={{0,1},{1,0},{2,3},{3,2},{4,5},{5,4},{6,7},{7,6},{8,9},{9,8},{10,11... | collective-permute-start | bytes 1179656 | tf_op jit(solution)/shard_map/ppermute | solution.py:18
  103.1 12.1 %collective-permute-start.9 = (bf16[256,512]{1,0:T(8,128)(2,1)S(1)}, bf16[256,512]{1,0:T(8,128)(2,1)S(1)}, u32[]{:S(2)}, u32[]{:S(2)}) collective-permute-start(bf16[256,512]{1,0:T(8,128)(2,1)S(1)} %slice.257), channel_id=1, source_target_pairs={{0,1},{1,0},{2,3},{3,2},{4,5},{5,4},{6,7},{7,6},{8,9},{9,8},{10,11... | collective-permute-start | bytes 786440 | tf_op jit(solution)/shard_map/ppermute | solution.py:18
  103.2 12.0 %collective-permute-start.8 = (bf16[256,512]{1,0:T(8,128)(2,1)S(1)}, bf16[256,512]{1,0:T(8,128)(2,1)S(1)}, u32[]{:S(2)}, u32[]{:S(2)}) collective-permute-start(bf16[256,512]{1,0:T(8,128)(2,1)S(1)} %slice.256), channel_id=1, source_target_pairs={{0,2},{1,3},{2,0},{3,1},{4,6},{5,7},{6,4},{7,5},{8,10},{9,11},{10,... | collective-permute-start | bytes 786440 | tf_op jit(solution)/shard_map/ppermute | solution.py:18
  106.6 12.6 %copy-start.10 = (bf16[512,512]{1,0:T(8,128)(2,1)S(1)}, bf16[512,512]{1,0:T(8,128)(2,1)}, u32[]{:S(2)}) copy-start(bf16[512,512]{1,0:T(8,128)(2,1)} %get-tuple-element.110) | copy-start | bytes 1572868
  106.6 12.6 %copy-start.11 = (bf16[512,512]{1,0:T(8,128)(2,1)S(1)}, bf16[512,512]{1,0:T(8,128)(2,1)}, u32[]{:S(2)}) copy-start(bf16[512,512]{1,0:T(8,128)(2,1)} %get-tuple-element.111) | copy-start | bytes 1572868
  106.7 12.6 %copy-start.12 = (bf16[512,512]{1,0:T(8,128)(2,1)S(1)}, bf16[512,512]{1,0:T(8,128)(2,1)}, u32[]{:S(2)}) copy-start(bf16[512,512]{1,0:T(8,128)(2,1)} %get-tuple-element.112) | copy-start | bytes 1572868
  106.7 12.6 %copy-start.13 = (bf16[512,512]{1,0:T(8,128)(2,1)S(1)}, bf16[512,512]{1,0:T(8,128)(2,1)}, u32[]{:S(2)}) copy-start(bf16[512,512]{1,0:T(8,128)(2,1)} %get-tuple-element.113) | copy-start | bytes 1572868
  109.6 25.3 %collective-permute-start.28 = (bf16[384,512]{1,0:T(8,128)(2,1)S(1)}, bf16[384,512]{1,0:T(8,128)(2,1)S(1)}, u32[]{:S(2)}, u32[]{:S(2)}) collective-permute-start(bf16[384,512]{1,0:T(8,128)(2,1)S(1)} %constant_dynamic-update-slice_fusion.2), channel_id=1, source_target_pairs={{0,1},{1,0},{2,3},{3,2},{4,5},{5,4},{6,7},{7,6},{8,9},{9,8},{10,11... | collective-permute-start | bytes 1179656 | tf_op jit(solution)/shard_map/ppermute | solution.py:18
  112.1 22.8 %collective-permute-start.27 = (bf16[384,512]{1,0:T(8,128)(2,1)S(1)}, bf16[384,512]{1,0:T(8,128)(2,1)S(1)}, u32[]{:S(2)}, u32[]{:S(2)}) collective-permute-start(bf16[384,512]{1,0:T(8,128)(2,1)S(1)} %constant_dynamic-update-slice_fusion.2), channel_id=1, source_target_pairs={{0,2},{1,3},{2,0},{3,1},{4,6},{5,7},{6,4},{7,5},{8,10},{9,11},{10,... | collective-permute-start | bytes 1179656 | tf_op jit(solution)/shard_map/ppermute | solution.py:18
  115.2 13.1 %collective-permute-start.19 = (bf16[192,512]{1,0:T(8,128)(2,1)S(1)}, bf16[192,512]{1,0:T(8,128)(2,1)S(1)}, u32[]{:S(2)}, u32[]{:S(2)}) collective-permute-start(bf16[192,512]{1,0:T(8,128)(2,1)S(1)} %slice.265), channel_id=1, source_target_pairs={{0,2},{1,3},{2,0},{3,1},{4,6},{5,7},{6,4},{7,5},{8,10},{9,11},{10,... | collective-permute-start | bytes 589832 | tf_op jit(solution)/shard_map/ppermute | solution.py:18
  116.7 11.5 %collective-permute-start.20 = (bf16[192,512]{1,0:T(8,128)(2,1)S(1)}, bf16[192,512]{1,0:T(8,128)(2,1)S(1)}, u32[]{:S(2)}, u32[]{:S(2)}) collective-permute-start(bf16[192,512]{1,0:T(8,128)(2,1)S(1)} %slice.266), channel_id=1, source_target_pairs={{0,1},{1,0},{2,3},{3,2},{4,5},{5,4},{6,7},{7,6},{8,9},{9,8},{10,11... | collective-permute-start | bytes 589832 | tf_op jit(solution)/shard_map/ppermute | solution.py:18
  128.3 7.2 %collective-permute-start.31 = (bf16[192,512]{1,0:T(8,128)(2,1)S(1)}, bf16[192,512]{1,0:T(8,128)(2,1)S(1)}, u32[]{:S(2)}, u32[]{:S(2)}) collective-permute-start(bf16[192,512]{1,0:T(8,128)(2,1)S(1)} %slice.273), channel_id=1, source_target_pairs={{0,2},{1,3},{2,0},{3,1},{4,6},{5,7},{6,4},{7,5},{8,10},{9,11},{10,... | collective-permute-start | bytes 589832 | tf_op jit(solution)/shard_map/ppermute | solution.py:18
  129.5 6.3 %collective-permute-start.32 = (bf16[192,512]{1,0:T(8,128)(2,1)S(1)}, bf16[192,512]{1,0:T(8,128)(2,1)S(1)}, u32[]{:S(2)}, u32[]{:S(2)}) collective-permute-start(bf16[192,512]{1,0:T(8,128)(2,1)S(1)} %slice.274), channel_id=1, source_target_pairs={{0,1},{1,0},{2,3},{3,2},{4,5},{5,4},{6,7},{7,6},{8,9},{9,8},{10,11... | collective-permute-start | bytes 589832 | tf_op jit(solution)/shard_map/ppermute | solution.py:18
  134.9 16.7 %collective-permute-start.30 = (bf16[384,512]{1,0:T(8,128)(2,1)S(1)}, bf16[384,512]{1,0:T(8,128)(2,1)S(1)}, u32[]{:S(2)}, u32[]{:S(2)}) collective-permute-start(bf16[384,512]{1,0:T(8,128)(2,1)S(1)} %fusion.160), channel_id=1, source_target_pairs={{0,2},{1,3},{2,0},{3,1},{4,6},{5,7},{6,4},{7,5},{8,10},{9,11},{10,... | collective-permute-start | bytes 1179656 | tf_op jit(solution)/shard_map/ppermute | solution.py:18
  135.4 16.1 %collective-permute-start.29 = (bf16[384,512]{1,0:T(8,128)(2,1)S(1)}, bf16[384,512]{1,0:T(8,128)(2,1)S(1)}, u32[]{:S(2)}, u32[]{:S(2)}) collective-permute-start(bf16[384,512]{1,0:T(8,128)(2,1)S(1)} %fusion.160), channel_id=1, source_target_pairs={{0,1},{1,0},{2,3},{3,2},{4,5},{5,4},{6,7},{7,6},{8,9},{9,8},{10,11... | collective-permute-start | bytes 1179656 | tf_op jit(solution)/shard_map/ppermute | solution.py:18
  135.8 14.9 %collective-permute-start.34 = (bf16[192,512]{1,0:T(8,128)(2,1)S(1)}, bf16[192,512]{1,0:T(8,128)(2,1)S(1)}, u32[]{:S(2)}, u32[]{:S(2)}) collective-permute-start(bf16[192,512]{1,0:T(8,128)(2,1)S(1)} %slice.272), channel_id=1, source_target_pairs={{0,1},{1,0},{2,3},{3,2},{4,5},{5,4},{6,7},{7,6},{8,9},{9,8},{10,11... | collective-permute-start | bytes 589832 | tf_op jit(solution)/shard_map/ppermute | solution.py:18
  138.1 12.6 %collective-permute-start.33 = (bf16[192,512]{1,0:T(8,128)(2,1)S(1)}, bf16[192,512]{1,0:T(8,128)(2,1)S(1)}, u32[]{:S(2)}, u32[]{:S(2)}) collective-permute-start(bf16[192,512]{1,0:T(8,128)(2,1)S(1)} %slice.271), channel_id=1, source_target_pairs={{0,2},{1,3},{2,0},{3,1},{4,6},{5,7},{6,4},{7,5},{8,10},{9,11},{10,... | collective-permute-start | bytes 589832 | tf_op jit(solution)/shard_map/ppermute | solution.py:18
  151.6 7.8 %collective-permute-start.35 = (bf16[192,512]{1,0:T(8,128)(2,1)S(1)}, bf16[192,512]{1,0:T(8,128)(2,1)S(1)}, u32[]{:S(2)}, u32[]{:S(2)}) collective-permute-start(bf16[192,512]{1,0:T(8,128)(2,1)S(1)} %slice.269), channel_id=1, source_target_pairs={{0,2},{1,3},{2,0},{3,1},{4,6},{5,7},{6,4},{7,5},{8,10},{9,11},{10,... | collective-permute-start | bytes 589832 | tf_op jit(solution)/shard_map/ppermute | solution.py:18
  153.2 7.8 %collective-permute-start.36 = (bf16[192,512]{1,0:T(8,128)(2,1)S(1)}, bf16[192,512]{1,0:T(8,128)(2,1)S(1)}, u32[]{:S(2)}, u32[]{:S(2)}) collective-permute-start(bf16[192,512]{1,0:T(8,128)(2,1)S(1)} %slice.270), channel_id=1, source_target_pairs={{0,1},{1,0},{2,3},{3,2},{4,5},{5,4},{6,7},{7,6},{8,9},{9,8},{10,11... | collective-permute-start | bytes 589832 | tf_op jit(solution)/shard_map/ppermute | solution.py:18
  155.3 12.4 %collective-permute-start.40 = (bf16[384,512]{1,0:T(8,128)(2,1)S(1)}, bf16[384,512]{1,0:T(8,128)(2,1)S(1)}, u32[]{:S(2)}, u32[]{:S(2)}) collective-permute-start(bf16[384,512]{1,0:T(8,128)(2,1)S(1)} %fusion.159), channel_id=1, source_target_pairs={{0,2},{1,3},{2,0},{3,1},{4,6},{5,7},{6,4},{7,5},{8,10},{9,11},{10,... | collective-permute-start | bytes 1179656 | tf_op jit(solution)/shard_map/ppermute | solution.py:18
  156.9 12.1 %collective-permute-start.39 = (bf16[384,512]{1,0:T(8,128)(2,1)S(1)}, bf16[384,512]{1,0:T(8,128)(2,1)S(1)}, u32[]{:S(2)}, u32[]{:S(2)}) collective-permute-start(bf16[384,512]{1,0:T(8,128)(2,1)S(1)} %fusion.159), channel_id=1, source_target_pairs={{0,1},{1,0},{2,3},{3,2},{4,5},{5,4},{6,7},{7,6},{8,9},{9,8},{10,11... | collective-permute-start | bytes 1179656 | tf_op jit(solution)/shard_map/ppermute | solution.py:18
  162.0 9.3 %collective-permute-start.37 = (bf16[192,512]{1,0:T(8,128)(2,1)S(1)}, bf16[192,512]{1,0:T(8,128)(2,1)S(1)}, u32[]{:S(2)}, u32[]{:S(2)}) collective-permute-start(bf16[192,512]{1,0:T(8,128)(2,1)S(1)} %get-tuple-element.117), channel_id=1, source_target_pairs={{0,24},{4,28},{8,16},{12,20},{16,8},{20,12},{24,0},{28,4},{1,25},{... | collective-permute-start | bytes 589832 | tf_op jit(solution)/shard_map/ppermute | solution.py:18
  166.4 8.0 %collective-permute-start.38 = (bf16[192,512]{1,0:T(8,128)(2,1)S(1)}, bf16[192,512]{1,0:T(8,128)(2,1)S(1)}, u32[]{:S(2)}, u32[]{:S(2)}) collective-permute-start(bf16[192,512]{1,0:T(8,128)(2,1)S(1)} %get-tuple-element.116), channel_id=1, source_target_pairs={{0,28},{4,24},{8,20},{12,16},{16,12},{20,8},{24,4},{28,0},{1,29},{... | collective-permute-start | bytes 589832 | tf_op jit(solution)/shard_map/ppermute | solution.py:18
  169.0 22.1 %collective-permute-start.46 = (bf16[384,512]{1,0:T(8,128)(2,1)S(1)}, bf16[384,512]{1,0:T(8,128)(2,1)S(1)}, u32[]{:S(2)}, u32[]{:S(2)}) collective-permute-start(bf16[384,512]{1,0:T(8,128)(2,1)S(1)} %fusion.158), channel_id=1, source_target_pairs={{0,2},{1,3},{2,0},{3,1},{4,6},{5,7},{6,4},{7,5},{8,10},{9,11},{10,... | collective-permute-start | bytes 1179656 | tf_op jit(solution)/shard_map/ppermute | solution.py:18
  169.5 21.6 %collective-permute-start.45 = (bf16[384,512]{1,0:T(8,128)(2,1)S(1)}, bf16[384,512]{1,0:T(8,128)(2,1)S(1)}, u32[]{:S(2)}, u32[]{:S(2)}) collective-permute-start(bf16[384,512]{1,0:T(8,128)(2,1)S(1)} %fusion.158), channel_id=1, source_target_pairs={{0,1},{1,0},{2,3},{3,2},{4,5},{5,4},{6,7},{7,6},{8,9},{9,8},{10,11... | collective-permute-start | bytes 1179656 | tf_op jit(solution)/shard_map/ppermute | solution.py:18
  170.5 13.4 %collective-permute-start.41 = (bf16[192,512]{1,0:T(8,128)(2,1)S(1)}, bf16[192,512]{1,0:T(8,128)(2,1)S(1)}, u32[]{:S(2)}, u32[]{:S(2)}) collective-permute-start(bf16[192,512]{1,0:T(8,128)(2,1)S(1)} %slice.280), channel_id=1, source_target_pairs={{0,2},{1,3},{2,0},{3,1},{4,6},{5,7},{6,4},{7,5},{8,10},{9,11},{10,... | collective-permute-start | bytes 589832 | tf_op jit(solution)/shard_map/ppermute | solution.py:18
  171.4 12.7 %collective-permute-start.42 = (bf16[192,512]{1,0:T(8,128)(2,1)S(1)}, bf16[192,512]{1,0:T(8,128)(2,1)S(1)}, u32[]{:S(2)}, u32[]{:S(2)}) collective-permute-start(bf16[192,512]{1,0:T(8,128)(2,1)S(1)} %slice.281), channel_id=1, source_target_pairs={{0,1},{1,0},{2,3},{3,2},{4,5},{5,4},{6,7},{7,6},{8,9},{9,8},{10,11... | collective-permute-start | bytes 589832 | tf_op jit(solution)/shard_map/ppermute | solution.py:18
  174.4 16.2 %copy-start.25 = (s32[384]{0:T(512)S(1)}, s32[384]{0:T(512)}, u32[]{:S(2)}) copy-start(s32[384]{0:T(512)} %copy-done.24) | copy-start | bytes 4612
  185.1 18.6 %collective-permute-start.43 = (bf16[192,512]{1,0:T(8,128)(2,1)S(1)}, bf16[192,512]{1,0:T(8,128)(2,1)S(1)}, u32[]{:S(2)}, u32[]{:S(2)}) collective-permute-start(bf16[192,512]{1,0:T(8,128)(2,1)S(1)} %get-tuple-element.119), channel_id=1, source_target_pairs={{0,16},{4,20},{8,24},{12,28},{16,0},{20,4},{24,8},{28,12},{1,17},{... | collective-permute-start | bytes 589832 | tf_op jit(solution)/shard_map/ppermute | solution.py:18
  190.6 16.1 %collective-permute-start.44 = (bf16[192,512]{1,0:T(8,128)(2,1)S(1)}, bf16[192,512]{1,0:T(8,128)(2,1)S(1)}, u32[]{:S(2)}, u32[]{:S(2)}) collective-permute-start(bf16[192,512]{1,0:T(8,128)(2,1)S(1)} %get-tuple-element.118), channel_id=1, source_target_pairs={{0,20},{4,16},{8,28},{12,24},{16,4},{20,0},{24,12},{28,8},{1,21},{... | collective-permute-start | bytes 589832 | tf_op jit(solution)/shard_map/ppermute | solution.py:18
  191.1 20.0 %collective-permute-start.51 = (bf16[384,512]{1,0:T(8,128)(2,1)S(1)}, bf16[384,512]{1,0:T(8,128)(2,1)S(1)}, u32[]{:S(2)}, u32[]{:S(2)}) collective-permute-start(bf16[384,512]{1,0:T(8,128)(2,1)S(1)} %fusion.157), channel_id=1, source_target_pairs={{0,1},{1,0},{2,3},{3,2},{4,5},{5,4},{6,7},{7,6},{8,9},{9,8},{10,11... | collective-permute-start | bytes 1179656 | tf_op jit(solution)/shard_map/ppermute | solution.py:18
  191.5 19.7 %collective-permute-start.52 = (bf16[384,512]{1,0:T(8,128)(2,1)S(1)}, bf16[384,512]{1,0:T(8,128)(2,1)S(1)}, u32[]{:S(2)}, u32[]{:S(2)}) collective-permute-start(bf16[384,512]{1,0:T(8,128)(2,1)S(1)} %fusion.157), channel_id=1, source_target_pairs={{0,2},{1,3},{2,0},{3,1},{4,6},{5,7},{6,4},{7,5},{8,10},{9,11},{10,... | collective-permute-start | bytes 1179656 | tf_op jit(solution)/shard_map/ppermute | solution.py:18
  191.9 15.4 %collective-permute-start.48 = (bf16[192,512]{1,0:T(8,128)(2,1)S(1)}, bf16[192,512]{1,0:T(8,128)(2,1)S(1)}, u32[]{:S(2)}, u32[]{:S(2)}) collective-permute-start(bf16[192,512]{1,0:T(8,128)(2,1)S(1)} %slice.287), channel_id=1, source_target_pairs={{0,1},{1,0},{2,3},{3,2},{4,5},{5,4},{6,7},{7,6},{8,9},{9,8},{10,11... | collective-permute-start | bytes 589832 | tf_op jit(solution)/shard_map/ppermute | solution.py:18
  203.8 5.7 %collective-permute-start.47 = (bf16[192,512]{1,0:T(8,128)(2,1)S(1)}, bf16[192,512]{1,0:T(8,128)(2,1)S(1)}, u32[]{:S(2)}, u32[]{:S(2)}) collective-permute-start(bf16[192,512]{1,0:T(8,128)(2,1)S(1)} %slice.286), channel_id=1, source_target_pairs={{0,2},{1,3},{2,0},{3,1},{4,6},{5,7},{6,4},{7,5},{8,10},{9,11},{10,... | collective-permute-start | bytes 589832 | tf_op jit(solution)/shard_map/ppermute | solution.py:18
  210.5 7.3 %collective-permute-start.49 = (bf16[192,512]{1,0:T(8,128)(2,1)S(1)}, bf16[192,512]{1,0:T(8,128)(2,1)S(1)}, u32[]{:S(2)}, u32[]{:S(2)}) collective-permute-start(bf16[192,512]{1,0:T(8,128)(2,1)S(1)} %get-tuple-element.121), channel_id=1, source_target_pairs={{0,8},{4,12},{8,0},{12,4},{16,24},{20,28},{24,16},{28,20},{1,9},{5... | collective-permute-start | bytes 589832 | tf_op jit(solution)/shard_map/ppermute | solution.py:18
  210.5 7.4 %collective-permute-start.50 = (bf16[192,512]{1,0:T(8,128)(2,1)S(1)}, bf16[192,512]{1,0:T(8,128)(2,1)S(1)}, u32[]{:S(2)}, u32[]{:S(2)}) collective-permute-start(bf16[192,512]{1,0:T(8,128)(2,1)S(1)} %get-tuple-element.120), channel_id=1, source_target_pairs={{0,12},{4,8},{8,4},{12,0},{16,28},{20,24},{24,20},{28,16},{1,13},{... | collective-permute-start | bytes 589832 | tf_op jit(solution)/shard_map/ppermute | solution.py:18
  211.2 7.3 %collective-permute-start.54 = (bf16[192,512]{1,0:T(8,128)(2,1)S(1)}, bf16[192,512]{1,0:T(8,128)(2,1)S(1)}, u32[]{:S(2)}, u32[]{:S(2)}) collective-permute-start(bf16[192,512]{1,0:T(8,128)(2,1)S(1)} %slice.293), channel_id=1, source_target_pairs={{0,1},{1,0},{2,3},{3,2},{4,5},{5,4},{6,7},{7,6},{8,9},{9,8},{10,11... | collective-permute-start | bytes 589832 | tf_op jit(solution)/shard_map/ppermute | solution.py:18
  212.5 7.0 %collective-permute-start.53 = (bf16[192,512]{1,0:T(8,128)(2,1)S(1)}, bf16[192,512]{1,0:T(8,128)(2,1)S(1)}, u32[]{:S(2)}, u32[]{:S(2)}) collective-permute-start(bf16[192,512]{1,0:T(8,128)(2,1)S(1)} %slice.292), channel_id=1, source_target_pairs={{0,2},{1,3},{2,0},{3,1},{4,6},{5,7},{6,4},{7,5},{8,10},{9,11},{10,... | collective-permute-start | bytes 589832 | tf_op jit(solution)/shard_map/ppermute | solution.py:18
  220.5 1.9 collective-permute-start.55
  (22 other events, 87.7 us)
where the time goes:
time: 226 us; the launch traced here: 225 us
  waiting for transfers between devices  99.9 us (44%)
  starting transfers between devices  70.9 us (31%)
  matrix products  24.1 us (11%)
  other arithmetic  14.4 us (6%)
  local copies, waits for them, and re-layouts  14.3 us (6%)
    ppermute x54, waiting for transfers between devices, swapped(): return lax.ppermute(block, axis, [(i, i ^ bits) for i in range(count)])  99.6 us
    ppermute x54, starting transfers between devices, swapped(): return lax.ppermute(block, axis, [(i, i ^ bits) for i in range(count)])  66.4 us
    dot_general x24, matrix products, dot(): lax.dot_general(a, b, (((1,), (0,)), ((), ())), preferred_element_type=jn...  24.1 us
    reduce_sum x5, other arithmetic, layer_norm(): center = values - jnp.mean(values, axis=-1, keepdims=True)  6.15 us
    dynamic_slice x4, local copies, waits for them, and re-layouts, arranged(): lax.dynamic_slice_in_dim(weight, (tp_index ^ j) * width, width, 0)  5.87 us
  transfers between devices with their start and end apart: 56, of which 26 were waited for; matrix products, arithmetic and copies ran while one was open for 21% of the time, Pallas kernels for 0%

commit v1 on v0

--- a/solution.py
+++ b/solution.py
@@ -23,8 +23,8 @@
         self.past = []
 
     def exchange(self, to_second, to_first):
-        if len(self.past) > 1:
-            to_second, to_first, *_ = lax.optimization_barrier((to_second, to_first, *self.past[-2]))
+        if len(self.past) > 2:
+            to_second, to_first, *_ = lax.optimization_barrier((to_second, to_first, *self.past[-3]))
         result = (swapped(to_second, "tp", 2), swapped(to_first, "tp", 1))
         self.past.append(result)
         return result
@@ -40,7 +40,8 @@
             return lax.all_gather(begun, "tp", axis=1, tiled=True)
         block, first, second = begun
         half = block.shape[0] // 2
-        top, bottom = self.exchange(first[:half], second[half:])
+        upper, lower = first[:half], second[half:]
+        top, bottom = self.exchange(upper, lower)
         return jnp.concatenate([block, first, second, jnp.concatenate([top, bottom], axis=0)], axis=1)
 
 

time: 226 us -> 222 us (0.982)
  starting transfers between devices: 70.9 us -> 61.5 us
  other arithmetic: 14.4 us -> 18.3 us
  waiting for transfers between devices: 99.9 us -> 103 us
    ppermute x54, starting transfers between devices: 66.4 us -> 57 us  [swapped(): return lax.ppermute(block, axis, [(i, i ^ bits) for i in range(count)])]
    ppermute x54, waiting for transfers between devices: 99.6 us -> 103 us  [swapped(): return lax.ppermute(block, axis, [(i, i ^ bits) for i in range(count)])]
  transfers between devices with their start and end apart: 56 -> 56, of which waited for: 26 -> 31; matrix products, arithmetic and copies ran while one was open for 21% -> 23% of each run, Pallas kernels for 0% -> 0%
where the time goes in v1:
time: 222 us; the launch traced here: 221 us
  waiting for transfers between devices  103 us (46%)
  starting transfers between devices  61.5 us (28%)
  matrix products  22.9 us (10%)
  other arithmetic  18.3 us (8%)
  local copies, waits for them, and re-layouts  14.4 us (6%)
    ppermute x54, waiting for transfers between devices, swapped(): return lax.ppermute(block, axis, [(i, i ^ bits) for i in range(count)])  103 us
    ppermute x54, starting transfers between devices, swapped(): return lax.ppermute(block, axis, [(i, i ^ bits) for i in range(count)])  57 us
    dot_general x24, matrix products, dot(): lax.dot_general(a, b, (((1,), (0,)), ((), ())), preferred_element_type=jn...  22.9 us
    reduce_sum x5, other arithmetic, layer_norm(): center = values - jnp.mean(values, axis=-1, keepdims=True)  8.27 us
  transfers between devices with their start and end apart: 56, of which 31 were waited for; matrix products, arithmetic and copies ran while one was open for 23% of the time, Pallas kernels for 0%

profile of v1, /device:TPU:0, one launch (start us, length us, event | category | flops | bytes accessed | tf_op | source)
XLA Modules:
  0.0 221.3 jit_solution(5177608776028792583)
XLA Ops:
  0.6 3.1 %collective-permute-start.1 = (bf16[512,512]{1,0:T(8,128)(2,1)}, bf16[512,512]{1,0:T(8,128)(2,1)S(1)}, u32[]{:S(2)}, u32[]{:S(2)}) collective-permute-start(bf16[512,512]{1,0:T(8,128)(2,1)} %param.12), channel_id=1, source_target_pairs={{0,2},{1,3},{2,0},{3,1},{4,6},{5,7},{6,4},{7,5},{8,10},{9,11},{10,... | collective-permute-start | bytes 1572872 | tf_op jit(solution)/shard_map/ppermute | solution.py:18
  3.7 1.5 collective-permute-start
  9.9 3.6 %collective-permute-start.15 = (bf16[192,512]{1,0:T(8,128)(2,1)}, bf16[192,512]{1,0:T(8,128)(2,1)}, u32[]{:S(2)}, u32[]{:S(2)}) collective-permute-start(bf16[192,512]{1,0:T(8,128)(2,1)} %get-tuple-element.125), channel_id=1, source_target_pairs={{0,24},{4,28},{8,16},{12,20},{16,8},{20,12},{24,0},{28,4},{1,25},{... | collective-permute-start | bytes 589832 | tf_op jit(solution)/shard_map/ppermute | solution.py:18
  15.4 1.4 constant_dynamic-slice_fusion.3
  16.7 1.0 copy-done.4
  17.7 1.4 constant_dynamic-slice_fusion.7
  19.1 1.5 fusion.236
  20.6 1.1 convolution_convert_fusion.1
  22.5 1.4 dynamic-slice_bitcast_fusion.3
  25.5 2.1 fusion.153
  28.6 3.4 %collective-permute-start.39 = (bf16[192,512]{1,0:T(8,128)(2,1)S(1)}, bf16[192,512]{1,0:T(8,128)(2,1)S(1)}, u32[]{:S(2)}, u32[]{:S(2)}) collective-permute-start(bf16[192,512]{1,0:T(8,128)(2,1)S(1)} %get-tuple-element.119), channel_id=1, source_target_pairs={{0,8},{4,12},{8,0},{12,4},{16,24},{20,28},{24,16},{28,20},{1,9},{5... | collective-permute-start | bytes 589832 | tf_op jit(solution)/shard_map/ppermute | solution.py:18
  33.0 7.1 %collective-permute-done.27 = bf16[192,512]{1,0:T(8,128)(2,1)S(1)} collective-permute-done((bf16[192,512]{1,0:T(8,128)(2,1)S(1)}, bf16[192,512]{1,0:T(8,128)(2,1)S(1)}, u32[]{:S(2)}, u32[]{:S(2)}) %collective-permute-start.27) | collective-permute-done | bytes 196640 | tf_op jit(solution)/shard_map/ppermute | solution.py:18
  41.2 1.8 collective-permute-start.40
  44.1 1.6 collective-permute-start.3
  45.6 5.7 %collective-permute-done.28 = bf16[192,512]{1,0:T(8,128)(2,1)S(1)} collective-permute-done((bf16[192,512]{1,0:T(8,128)(2,1)S(1)}, bf16[192,512]{1,0:T(8,128)(2,1)S(1)}, u32[]{:S(2)}, u32[]{:S(2)}) %collective-permute-start.28) | collective-permute-done | bytes 196640 | tf_op jit(solution)/shard_map/ppermute | solution.py:18
  52.8 1.6 collective-permute-start.11
  54.4 1.0 collective-permute-start.12
  55.4 1.2 collective-permute-done.3
  56.6 3.8 %collective-permute-done.2 = bf16[256,512]{1,0:T(8,128)(2,1)S(1)} collective-permute-done((bf16[256,512]{1,0:T(8,128)(2,1)S(1)}, bf16[256,512]{1,0:T(8,128)(2,1)S(1)}, u32[]{:S(2)}, u32[]{:S(2)}) %collective-permute-start.2) | collective-permute-done | bytes 262176 | tf_op jit(solution)/shard_map/ppermute | solution.py:18
  60.5 6.9 %convert_reduce_fusion = (f32[512]{0:T(512)S(1)}, bf16[512,2048]{1,0:T(8,128)(2,1)S(1)}) fusion(bf16[256,512]{1,0:T(8,128)(2,1)S(1)} %collective-permute-done.3, bf16[256,512]{1,0:T(8,128)(2,1)S(1)} %collective-permute-done.2, bf16[512,512]{1,0:T(8,128)(2,1)S(1)} %collective-permute-done.1, bf16[512,512]{1,0:T(8,128)(2,1)} %collective-permute-done, ...), kind=kLoop, calls=%fused_computation.9 | loop fusion | flops 12582400 | bytes 4196352 | tf_op jit(solution)/shard_map/reduce_sum | solution.py:64
  68.9 1.3 fusion.135
  70.2 1.3 collective-permute-start.5
  71.5 3.2 %collective-permute-start.4 = (bf16[8,512]{1,0:T(8,128)(2,1)S(1)}, bf16[8,512]{1,0:T(8,128)(2,1)S(1)}, u32[]{:S(2)}, u32[]{:S(2)}) collective-permute-start(bf16[8,512]{1,0:T(8,128)(2,1)S(1)} %get-tuple-element.110), channel_id=1, source_target_pairs={{0,4},{4,8},{8,12},{12,16},{16,20},{20,24},{24,28},{1,5},{5,9},{9,... | collective-permute-start | bytes 24584 | tf_op jit(solution)/shard_map/ppermute | solution.py:73
  77.4 1.6 collective-permute-start.9
  79.0 1.5 collective-permute-start.10
  80.5 1.9 fusion.60
  82.4 4.4 %collective-permute-done.17 = bf16[384,512]{1,0:T(8,128)(2,1)S(1)} collective-permute-done((bf16[384,512]{1,0:T(8,128)(2,1)S(1)}, bf16[384,512]{1,0:T(8,128)(2,1)S(1)}, u32[]{:S(2)}, u32[]{:S(2)}) %collective-permute-start.17) | collective-permute-done | bytes 393248 | tf_op jit(solution)/shard_map/ppermute | solution.py:18
  87.4 1.6 collective-permute-start.20
  89.7 8.4 %collective-permute-done.9 = bf16[512,512]{1,0:T(8,128)(2,1)S(1)} collective-permute-done((bf16[512,512]{1,0:T(8,128)(2,1)S(1)}, bf16[512,512]{1,0:T(8,128)(2,1)S(1)}, u32[]{:S(2)}, u32[]{:S(2)}) %collective-permute-start.9) | collective-permute-done | bytes 524320 | tf_op jit(solution)/shard_map/ppermute | solution.py:18
  98.6 1.6 collective-permute-start.14
  101.2 1.1 collective-permute-done.20
  103.7 1.9 fusion.54
  105.8 1.6 collective-permute-start.21
  109.9 6.4 %collective-permute-done.29 = bf16[384,512]{1,0:T(8,128)(2,1)S(1)} collective-permute-done((bf16[384,512]{1,0:T(8,128)(2,1)S(1)}, bf16[384,512]{1,0:T(8,128)(2,1)S(1)}, u32[]{:S(2)}, u32[]{:S(2)}) %collective-permute-start.29) | collective-permute-done | bytes 393248 | tf_op jit(solution)/shard_map/ppermute | solution.py:18
  116.3 1.4 collective-permute-done.30
  118.9 2.1 fusion.130
  121.0 3.7 %collective-permute-done.21 = bf16[384,512]{1,0:T(8,128)(2,1)S(1)} collective-permute-done((bf16[384,512]{1,0:T(8,128)(2,1)S(1)}, bf16[384,512]{1,0:T(8,128)(2,1)S(1)}, u32[]{:S(2)}, u32[]{:S(2)}) %collective-permute-start.21) | collective-permute-done | bytes 393248 | tf_op jit(solution)/shard_map/ppermute | solution.py:18
  126.9 9.5 %collective-permute-done.32 = bf16[192,512]{1,0:T(8,128)(2,1)S(1)} collective-permute-done((bf16[192,512]{1,0:T(8,128)(2,1)S(1)}, bf16[192,512]{1,0:T(8,128)(2,1)S(1)}, u32[]{:S(2)}, u32[]{:S(2)}) %collective-permute-start.32) | collective-permute-done | bytes 196640 | tf_op jit(solution)/shard_map/ppermute | solution.py:18
  137.9 1.9 fusion.56
  139.7 1.1 collective-permute-done.23
  140.9 1.5 collective-permute-done.24
  145.8 1.4 collective-permute-start.34
  147.3 2.0 collective-permute-start.51
  149.2 3.9 %collective-permute-done.25 = bf16[192,512]{1,0:T(8,128)(2,1)S(1)} collective-permute-done((bf16[192,512]{1,0:T(8,128)(2,1)S(1)}, bf16[192,512]{1,0:T(8,128)(2,1)S(1)}, u32[]{:S(2)}, u32[]{:S(2)}) %collective-permute-start.25) | collective-permute-done | bytes 196640 | tf_op jit(solution)/shard_map/ppermute | solution.py:18
  153.2 1.4 collective-permute-start.43
  155.2 13.2 %collective-permute-done.44 = bf16[192,512]{1,0:T(8,128)(2,1)S(1)} collective-permute-done((bf16[192,512]{1,0:T(8,128)(2,1)S(1)}, bf16[192,512]{1,0:T(8,128)(2,1)S(1)}, u32[]{:S(2)}, u32[]{:S(2)}) %collective-permute-start.44) | collective-permute-done | bytes 196640 | tf_op jit(solution)/shard_map/ppermute | solution.py:18
  168.4 2.3 %collective-permute-start.52 = (bf16[384,512]{1,0:T(8,128)(2,1)S(1)}, bf16[384,512]{1,0:T(8,128)(2,1)S(1)}, u32[]{:S(2)}, u32[]{:S(2)}) collective-permute-start(bf16[384,512]{1,0:T(8,128)(2,1)S(1)} %fusion.157), channel_id=1, source_target_pairs={{0,2},{1,3},{2,0},{3,1},{4,6},{5,7},{6,4},{7,5},{8,10},{9,11},{10,... | collective-permute-start | bytes 1179656 | tf_op jit(solution)/shard_map/ppermute | solution.py:18
  171.7 1.9 fusion.58
  174.6 1.5 collective-permute-start.45
  176.2 1.9 collective-permute-start.46
  178.2 2.3 %collective-permute-done.52 = bf16[384,512]{1,0:T(8,128)(2,1)S(1)} collective-permute-done((bf16[384,512]{1,0:T(8,128)(2,1)S(1)}, bf16[384,512]{1,0:T(8,128)(2,1)S(1)}, u32[]{:S(2)}, u32[]{:S(2)}) %collective-permute-start.52) | collective-permute-done | bytes 393248 | tf_op jit(solution)/shard_map/ppermute | solution.py:18
  180.4 4.2 %collective-permute-done.35 = bf16[192,512]{1,0:T(8,128)(2,1)S(1)} collective-permute-done((bf16[192,512]{1,0:T(8,128)(2,1)S(1)}, bf16[192,512]{1,0:T(8,128)(2,1)S(1)}, u32[]{:S(2)}, u32[]{:S(2)}) %collective-permute-start.35) | collective-permute-done | bytes 196640 | tf_op jit(solution)/shard_map/ppermute | solution.py:18
  185.4 1.5 collective-permute-start.53
  187.9 1.2 collective-permute-start.37
  190.1 3.0 %collective-permute-done.46 = bf16[384,512]{1,0:T(8,128)(2,1)S(1)} collective-permute-done((bf16[384,512]{1,0:T(8,128)(2,1)S(1)}, bf16[384,512]{1,0:T(8,128)(2,1)S(1)}, u32[]{:S(2)}, u32[]{:S(2)}) %collective-permute-start.46) | collective-permute-done | bytes 393248 | tf_op jit(solution)/shard_map/ppermute | solution.py:18
  193.9 1.7 collective-permute-start.47
  195.6 1.7 collective-permute-done.53
  197.3 1.0 fusion.140
  198.7 4.2 %collective-permute-done.37 = bf16[192,512]{1,0:T(8,128)(2,1)S(1)} collective-permute-done((bf16[192,512]{1,0:T(8,128)(2,1)S(1)}, bf16[192,512]{1,0:T(8,128)(2,1)S(1)}, u32[]{:S(2)}, u32[]{:S(2)}) %collective-permute-start.37) | collective-permute-done | bytes 196640 | tf_op jit(solution)/shard_map/ppermute | solution.py:18
  203.0 1.6 collective-permute-done.38
  207.6 1.6 collective-permute-start.50
  210.2 4.2 %collective-permute-done.49 = bf16[192,512]{1,0:T(8,128)(2,1)S(1)} collective-permute-done((bf16[192,512]{1,0:T(8,128)(2,1)S(1)}, bf16[192,512]{1,0:T(8,128)(2,1)S(1)}, u32[]{:S(2)}, u32[]{:S(2)}) %collective-permute-start.49) | collective-permute-done | bytes 196640 | tf_op jit(solution)/shard_map/ppermute | solution.py:18
  214.4 4.3 %collective-permute-done.50 = bf16[192,512]{1,0:T(8,128)(2,1)S(1)} collective-permute-done((bf16[192,512]{1,0:T(8,128)(2,1)S(1)}, bf16[192,512]{1,0:T(8,128)(2,1)S(1)}, u32[]{:S(2)}, u32[]{:S(2)}) %collective-permute-start.50) | collective-permute-done | bytes 196640 | tf_op jit(solution)/shard_map/ppermute | solution.py:18
  219.7 1.5 fusion.126
  (224 shorter events, 45.4 us)
Async XLA Ops:
  0.6 40.1 %collective-permute-start.1 = (bf16[512,512]{1,0:T(8,128)(2,1)}, bf16[512,512]{1,0:T(8,128)(2,1)S(1)}, u32[]{:S(2)}, u32[]{:S(2)}) collective-permute-start(bf16[512,512]{1,0:T(8,128)(2,1)} %param.12), channel_id=1, source_target_pairs={{0,2},{1,3},{2,0},{3,1},{4,6},{5,7},{6,4},{7,5},{8,10},{9,11},{10,... | collective-permute-start | bytes 1572872 | tf_op jit(solution)/shard_map/ppermute | solution.py:18
  3.7 37.5 %collective-permute-start = (bf16[512,512]{1,0:T(8,128)(2,1)}, bf16[512,512]{1,0:T(8,128)(2,1)}, u32[]{:S(2)}, u32[]{:S(2)}) collective-permute-start(bf16[512,512]{1,0:T(8,128)(2,1)} %param.12), channel_id=1, source_target_pairs={{0,1},{1,0},{2,3},{3,2},{4,5},{5,4},{6,7},{7,6},{8,9},{9,8},{10,11... | collective-permute-start | bytes 1572872 | tf_op jit(solution)/shard_map/ppermute | solution.py:18
  8.7 19.0 %collective-permute-start.6 = (bf16[192,512]{1,0:T(8,128)(2,1)}, bf16[192,512]{1,0:T(8,128)(2,1)S(1)}, u32[]{:S(2)}, u32[]{:S(2)}) collective-permute-start(bf16[192,512]{1,0:T(8,128)(2,1)} %get-tuple-element.127), channel_id=1, source_target_pairs={{0,4},{4,0},{8,12},{12,8},{16,20},{20,16},{24,28},{28,24},{1,5},{5... | collective-permute-start | bytes 589832 | tf_op jit(solution)/shard_map/ppermute | solution.py:18
  9.9 18.7 %collective-permute-start.15 = (bf16[192,512]{1,0:T(8,128)(2,1)}, bf16[192,512]{1,0:T(8,128)(2,1)}, u32[]{:S(2)}, u32[]{:S(2)}) collective-permute-start(bf16[192,512]{1,0:T(8,128)(2,1)} %get-tuple-element.125), channel_id=1, source_target_pairs={{0,24},{4,28},{8,16},{12,20},{16,8},{20,12},{24,0},{28,4},{1,25},{... | collective-permute-start | bytes 589832 | tf_op jit(solution)/shard_map/ppermute | solution.py:18
  13.5 30.5 %collective-permute-start.16 = (bf16[192,512]{1,0:T(8,128)(2,1)}, bf16[192,512]{1,0:T(8,128)(2,1)}, u32[]{:S(2)}, u32[]{:S(2)}) collective-permute-start(bf16[192,512]{1,0:T(8,128)(2,1)} %get-tuple-element.124), channel_id=1, source_target_pairs={{0,28},{4,24},{8,20},{12,16},{16,12},{20,8},{24,4},{28,0},{1,29},{... | collective-permute-start | bytes 589832 | tf_op jit(solution)/shard_map/ppermute | solution.py:18
  25.5 14.5 %copy-start.19 = (bf16[192,512]{1,0:T(8,128)(2,1)S(1)}, bf16[192,512]{1,0:T(8,128)(2,1)}, u32[]{:S(2)}) copy-start(bf16[192,512]{1,0:T(8,128)(2,1)} %get-tuple-element.122) | copy-start | bytes 589828
  27.6 13.6 %copy-start.20 = (bf16[192,512]{1,0:T(8,128)(2,1)S(1)}, bf16[192,512]{1,0:T(8,128)(2,1)}, u32[]{:S(2)}) copy-start(bf16[192,512]{1,0:T(8,128)(2,1)} %get-tuple-element.118) | copy-start | bytes 589828
  27.7 12.3 %collective-permute-start.27 = (bf16[192,512]{1,0:T(8,128)(2,1)S(1)}, bf16[192,512]{1,0:T(8,128)(2,1)S(1)}, u32[]{:S(2)}, u32[]{:S(2)}) collective-permute-start(bf16[192,512]{1,0:T(8,128)(2,1)S(1)} %copy-done.21), channel_id=1, source_target_pairs={{0,16},{4,20},{8,24},{12,28},{16,0},{20,4},{24,8},{28,12},{1,17},{... | collective-permute-start | bytes 589832 | tf_op jit(solution)/shard_map/ppermute | solution.py:18
  28.6 31.9 %copy-start.6 = (bf16[512,512]{1,0:T(8,128)(2,1)S(1)}, bf16[512,512]{1,0:T(8,128)(2,1)}, u32[]{:S(2)}) copy-start(bf16[512,512]{1,0:T(8,128)(2,1)} %param.12) | copy-start | bytes 1572868
  28.6 11.7 %collective-permute-start.39 = (bf16[192,512]{1,0:T(8,128)(2,1)S(1)}, bf16[192,512]{1,0:T(8,128)(2,1)S(1)}, u32[]{:S(2)}, u32[]{:S(2)}) collective-permute-start(bf16[192,512]{1,0:T(8,128)(2,1)S(1)} %get-tuple-element.119), channel_id=1, source_target_pairs={{0,8},{4,12},{8,0},{12,4},{16,24},{20,28},{24,16},{28,20},{1,9},{5... | collective-permute-start | bytes 589832 | tf_op jit(solution)/shard_map/ppermute | solution.py:18
  40.0 11.2 %collective-permute-start.28 = (bf16[192,512]{1,0:T(8,128)(2,1)S(1)}, bf16[192,512]{1,0:T(8,128)(2,1)S(1)}, u32[]{:S(2)}, u32[]{:S(2)}) collective-permute-start(bf16[192,512]{1,0:T(8,128)(2,1)S(1)} %copy-done.19), channel_id=1, source_target_pairs={{0,20},{4,16},{8,28},{12,24},{16,4},{20,0},{24,12},{28,8},{1,21},{... | collective-permute-start | bytes 589832 | tf_op jit(solution)/shard_map/ppermute | solution.py:18
  40.2 12.6 %collective-permute-start.7 = (bf16[384,512]{1,0:T(8,128)(2,1)S(1)}, bf16[384,512]{1,0:T(8,128)(2,1)S(1)}, u32[]{:S(2)}, u32[]{:S(2)}) collective-permute-start(bf16[384,512]{1,0:T(8,128)(2,1)S(1)} %pad_maximum_fusion.2), channel_id=1, source_target_pairs={{0,2},{1,3},{2,0},{3,1},{4,6},{5,7},{6,4},{7,5},{8,10},{9,11},{10,... | collective-permute-start | bytes 1179656 | tf_op jit(solution)/shard_map/ppermute | solution.py:18
  40.8 12.0 %collective-permute-start.8 = (bf16[384,512]{1,0:T(8,128)(2,1)S(1)}, bf16[384,512]{1,0:T(8,128)(2,1)S(1)}, u32[]{:S(2)}, u32[]{:S(2)}) collective-permute-start(bf16[384,512]{1,0:T(8,128)(2,1)S(1)} %pad_maximum_fusion.2), channel_id=1, source_target_pairs={{0,1},{1,0},{2,3},{3,2},{4,5},{5,4},{6,7},{7,6},{8,9},{9,8},{10,11... | collective-permute-start | bytes 1179656 | tf_op jit(solution)/shard_map/ppermute | solution.py:18
  41.2 11.5 %collective-permute-start.40 = (bf16[192,512]{1,0:T(8,128)(2,1)S(1)}, bf16[192,512]{1,0:T(8,128)(2,1)S(1)}, u32[]{:S(2)}, u32[]{:S(2)}) collective-permute-start(bf16[192,512]{1,0:T(8,128)(2,1)S(1)} %copy-done.20), channel_id=1, source_target_pairs={{0,12},{4,8},{8,4},{12,0},{16,28},{20,24},{24,20},{28,16},{1,13},{... | collective-permute-start | bytes 589832 | tf_op jit(solution)/shard_map/ppermute | solution.py:18
  44.1 12.6 %collective-permute-start.3 = (bf16[256,512]{1,0:T(8,128)(2,1)S(1)}, bf16[256,512]{1,0:T(8,128)(2,1)S(1)}, u32[]{:S(2)}, u32[]{:S(2)}) collective-permute-start(bf16[256,512]{1,0:T(8,128)(2,1)S(1)} %slice.253), channel_id=1, source_target_pairs={{0,1},{1,0},{2,3},{3,2},{4,5},{5,4},{6,7},{7,6},{8,9},{9,8},{10,11... | collective-permute-start | bytes 786440 | tf_op jit(solution)/shard_map/ppermute | solution.py:18
  51.3 9.2 %collective-permute-start.2 = (bf16[256,512]{1,0:T(8,128)(2,1)S(1)}, bf16[256,512]{1,0:T(8,128)(2,1)S(1)}, u32[]{:S(2)}, u32[]{:S(2)}) collective-permute-start(bf16[256,512]{1,0:T(8,128)(2,1)S(1)} %slice.252), channel_id=1, source_target_pairs={{0,2},{1,3},{2,0},{3,1},{4,6},{5,7},{6,4},{7,5},{8,10},{9,11},{10,... | collective-permute-start | bytes 786440 | tf_op jit(solution)/shard_map/ppermute | solution.py:18
  52.8 22.5 %collective-permute-start.11 = (bf16[192,512]{1,0:T(8,128)(2,1)S(1)}, bf16[192,512]{1,0:T(8,128)(2,1)S(1)}, u32[]{:S(2)}, u32[]{:S(2)}) collective-permute-start(bf16[192,512]{1,0:T(8,128)(2,1)S(1)} %slice.262), channel_id=1, source_target_pairs={{0,2},{1,3},{2,0},{3,1},{4,6},{5,7},{6,4},{7,5},{8,10},{9,11},{10,... | collective-permute-start | bytes 589832 | tf_op jit(solution)/shard_map/ppermute | solution.py:18
  54.4 21.4 %collective-permute-start.12 = (bf16[192,512]{1,0:T(8,128)(2,1)S(1)}, bf16[192,512]{1,0:T(8,128)(2,1)S(1)}, u32[]{:S(2)}, u32[]{:S(2)}) collective-permute-start(bf16[192,512]{1,0:T(8,128)(2,1)S(1)} %slice.263), channel_id=1, source_target_pairs={{0,1},{1,0},{2,3},{3,2},{4,5},{5,4},{6,7},{7,6},{8,9},{9,8},{10,11... | collective-permute-start | bytes 589832 | tf_op jit(solution)/shard_map/ppermute | solution.py:18
  70.2 6.5 %collective-permute-start.5 = (bf16[8,512]{1,0:T(8,128)(2,1)S(1)}, bf16[8,512]{1,0:T(8,128)(2,1)S(1)}, u32[]{:S(2)}, u32[]{:S(2)}) collective-permute-start(bf16[8,512]{1,0:T(8,128)(2,1)S(1)} %get-tuple-element.111), channel_id=1, source_target_pairs={{4,0},{8,4},{12,8},{16,12},{20,16},{24,20},{28,24},{5,1},{9,5},{13... | collective-permute-start | bytes 24584 | tf_op jit(solution)/shard_map/ppermute | solution.py:74
  71.5 5.2 %collective-permute-start.4 = (bf16[8,512]{1,0:T(8,128)(2,1)S(1)}, bf16[8,512]{1,0:T(8,128)(2,1)S(1)}, u32[]{:S(2)}, u32[]{:S(2)}) collective-permute-start(bf16[8,512]{1,0:T(8,128)(2,1)S(1)} %get-tuple-element.110), channel_id=1, source_target_pairs={{0,4},{4,8},{8,12},{12,16},{16,20},{20,24},{24,28},{1,5},{5,9},{9,... | collective-permute-start | bytes 24584 | tf_op jit(solution)/shard_map/ppermute | solution.py:73
  74.8 12.1 %collective-permute-start.17 = (bf16[384,512]{1,0:T(8,128)(2,1)S(1)}, bf16[384,512]{1,0:T(8,128)(2,1)S(1)}, u32[]{:S(2)}, u32[]{:S(2)}) collective-permute-start(bf16[384,512]{1,0:T(8,128)(2,1)S(1)} %constant_dynamic-update-slice_fusion), channel_id=1, source_target_pairs={{0,1},{1,0},{2,3},{3,2},{4,5},{5,4},{6,7},{7,6},{8,9},{9,8},{10,11... | collective-permute-start | bytes 1179656 | tf_op jit(solution)/shard_map/ppermute | solution.py:18
  75.4 12.0 %collective-permute-start.18 = (bf16[384,512]{1,0:T(8,128)(2,1)S(1)}, bf16[384,512]{1,0:T(8,128)(2,1)S(1)}, u32[]{:S(2)}, u32[]{:S(2)}) collective-permute-start(bf16[384,512]{1,0:T(8,128)(2,1)S(1)} %constant_dynamic-update-slice_fusion), channel_id=1, source_target_pairs={{0,2},{1,3},{2,0},{3,1},{4,6},{5,7},{6,4},{7,5},{8,10},{9,11},{10,... | collective-permute-start | bytes 1179656 | tf_op jit(solution)/shard_map/ppermute | solution.py:18
  77.4 20.6 %collective-permute-start.9 = (bf16[512,512]{1,0:T(8,128)(2,1)S(1)}, bf16[512,512]{1,0:T(8,128)(2,1)S(1)}, u32[]{:S(2)}, u32[]{:S(2)}) collective-permute-start(bf16[512,512]{1,0:T(8,128)(2,1)S(1)} %fusion.127), channel_id=1, source_target_pairs={{0,1},{1,0},{2,3},{3,2},{4,5},{5,4},{6,7},{7,6},{8,9},{9,8},{10,11... | collective-permute-start | bytes 1572872 | tf_op jit(solution)/shard_map/ppermute | solution.py:18
  79.0 19.6 %collective-permute-start.10 = (bf16[512,512]{1,0:T(8,128)(2,1)S(1)}, bf16[512,512]{1,0:T(8,128)(2,1)S(1)}, u32[]{:S(2)}, u32[]{:S(2)}) collective-permute-start(bf16[512,512]{1,0:T(8,128)(2,1)S(1)} %fusion.127), channel_id=1, source_target_pairs={{0,2},{1,3},{2,0},{3,1},{4,6},{5,7},{6,4},{7,5},{8,10},{9,11},{10,... | collective-permute-start | bytes 1572872 | tf_op jit(solution)/shard_map/ppermute | solution.py:18
  87.4 14.9 %collective-permute-start.20 = (bf16[192,512]{1,0:T(8,128)(2,1)S(1)}, bf16[192,512]{1,0:T(8,128)(2,1)S(1)}, u32[]{:S(2)}, u32[]{:S(2)}) collective-permute-start(bf16[192,512]{1,0:T(8,128)(2,1)S(1)} %slice.266), channel_id=1, source_target_pairs={{0,1},{1,0},{2,3},{3,2},{4,5},{5,4},{6,7},{7,6},{8,9},{9,8},{10,11... | collective-permute-start | bytes 589832 | tf_op jit(solution)/shard_map/ppermute | solution.py:18
  88.9 13.9 %collective-permute-start.19 = (bf16[192,512]{1,0:T(8,128)(2,1)S(1)}, bf16[192,512]{1,0:T(8,128)(2,1)S(1)}, u32[]{:S(2)}, u32[]{:S(2)}) collective-permute-start(bf16[192,512]{1,0:T(8,128)(2,1)S(1)} %slice.265), channel_id=1, source_target_pairs={{0,2},{1,3},{2,0},{3,1},{4,6},{5,7},{6,4},{7,5},{8,10},{9,11},{10,... | collective-permute-start | bytes 589832 | tf_op jit(solution)/shard_map/ppermute | solution.py:18
  98.6 9.3 %collective-permute-start.14 = (bf16[256,512]{1,0:T(8,128)(2,1)S(1)}, bf16[256,512]{1,0:T(8,128)(2,1)S(1)}, u32[]{:S(2)}, u32[]{:S(2)}) collective-permute-start(bf16[256,512]{1,0:T(8,128)(2,1)S(1)} %slice.261), channel_id=1, source_target_pairs={{0,1},{1,0},{2,3},{3,2},{4,5},{5,4},{6,7},{7,6},{8,9},{9,8},{10,11... | collective-permute-start | bytes 786440 | tf_op jit(solution)/shard_map/ppermute | solution.py:18
  100.2 9.2 %collective-permute-start.13 = (bf16[256,512]{1,0:T(8,128)(2,1)S(1)}, bf16[256,512]{1,0:T(8,128)(2,1)S(1)}, u32[]{:S(2)}, u32[]{:S(2)}) collective-permute-start(bf16[256,512]{1,0:T(8,128)(2,1)S(1)} %slice.260), channel_id=1, source_target_pairs={{0,2},{1,3},{2,0},{3,1},{4,6},{5,7},{6,4},{7,5},{8,10},{9,11},{10,... | collective-permute-start | bytes 786440 | tf_op jit(solution)/shard_map/ppermute | solution.py:18
  100.7 15.6 %collective-permute-start.29 = (bf16[384,512]{1,0:T(8,128)(2,1)S(1)}, bf16[384,512]{1,0:T(8,128)(2,1)S(1)}, u32[]{:S(2)}, u32[]{:S(2)}) collective-permute-start(bf16[384,512]{1,0:T(8,128)(2,1)S(1)} %constant_dynamic-update-slice_fusion.4), channel_id=1, source_target_pairs={{0,1},{1,0},{2,3},{3,2},{4,5},{5,4},{6,7},{7,6},{8,9},{9,8},{10,11... | collective-permute-start | bytes 1179656 | tf_op jit(solution)/shard_map/ppermute | solution.py:18
  102.3 15.5 %collective-permute-start.30 = (bf16[384,512]{1,0:T(8,128)(2,1)S(1)}, bf16[384,512]{1,0:T(8,128)(2,1)S(1)}, u32[]{:S(2)}, u32[]{:S(2)}) collective-permute-start(bf16[384,512]{1,0:T(8,128)(2,1)S(1)} %constant_dynamic-update-slice_fusion.4), channel_id=1, source_target_pairs={{0,2},{1,3},{2,0},{3,1},{4,6},{5,7},{6,4},{7,5},{8,10},{9,11},{10,... | collective-permute-start | bytes 1179656 | tf_op jit(solution)/shard_map/ppermute | solution.py:18
  105.5 13.4 %copy-start.11 = (bf16[512,512]{1,0:T(8,128)(2,1)S(1)}, bf16[512,512]{1,0:T(8,128)(2,1)}, u32[]{:S(2)}) copy-start(bf16[512,512]{1,0:T(8,128)(2,1)} %get-tuple-element.106) | copy-start | bytes 1572868
  105.6 13.4 %copy-start.12 = (bf16[512,512]{1,0:T(8,128)(2,1)S(1)}, bf16[512,512]{1,0:T(8,128)(2,1)}, u32[]{:S(2)}) copy-start(bf16[512,512]{1,0:T(8,128)(2,1)} %get-tuple-element.107) | copy-start | bytes 1572868
  105.6 13.4 %copy-start.13 = (bf16[512,512]{1,0:T(8,128)(2,1)S(1)}, bf16[512,512]{1,0:T(8,128)(2,1)}, u32[]{:S(2)}) copy-start(bf16[512,512]{1,0:T(8,128)(2,1)} %get-tuple-element.108) | copy-start | bytes 1572868
  105.6 13.3 %copy-start.14 = (bf16[512,512]{1,0:T(8,128)(2,1)S(1)}, bf16[512,512]{1,0:T(8,128)(2,1)}, u32[]{:S(2)}) copy-start(bf16[512,512]{1,0:T(8,128)(2,1)} %get-tuple-element.109) | copy-start | bytes 1572868
  105.8 18.9 %collective-permute-start.21 = (bf16[384,512]{1,0:T(8,128)(2,1)S(1)}, bf16[384,512]{1,0:T(8,128)(2,1)S(1)}, u32[]{:S(2)}, u32[]{:S(2)}) collective-permute-start(bf16[384,512]{1,0:T(8,128)(2,1)S(1)} %fusion.160), channel_id=1, source_target_pairs={{0,1},{1,0},{2,3},{3,2},{4,5},{5,4},{6,7},{7,6},{8,9},{9,8},{10,11... | collective-permute-start | bytes 1179656 | tf_op jit(solution)/shard_map/ppermute | solution.py:18
  107.9 18.3 %collective-permute-start.22 = (bf16[384,512]{1,0:T(8,128)(2,1)S(1)}, bf16[384,512]{1,0:T(8,128)(2,1)S(1)}, u32[]{:S(2)}, u32[]{:S(2)}) collective-permute-start(bf16[384,512]{1,0:T(8,128)(2,1)S(1)} %fusion.160), channel_id=1, source_target_pairs={{0,2},{1,3},{2,0},{3,1},{4,6},{5,7},{6,4},{7,5},{8,10},{9,11},{10,... | collective-permute-start | bytes 1179656 | tf_op jit(solution)/shard_map/ppermute | solution.py:18
  109.3 36.5 %collective-permute-start.41 = (bf16[384,512]{1,0:T(8,128)(2,1)S(1)}, bf16[384,512]{1,0:T(8,128)(2,1)S(1)}, u32[]{:S(2)}, u32[]{:S(2)}) collective-permute-start(bf16[384,512]{1,0:T(8,128)(2,1)S(1)} %constant_dynamic-update-slice_fusion.8), channel_id=1, source_target_pairs={{0,1},{1,0},{2,3},{3,2},{4,5},{5,4},{6,7},{7,6},{8,9},{9,8},{10,11... | collective-permute-start | bytes 1179656 | tf_op jit(solution)/shard_map/ppermute | solution.py:18
  117.8 18.6 %collective-permute-start.32 = (bf16[192,512]{1,0:T(8,128)(2,1)S(1)}, bf16[192,512]{1,0:T(8,128)(2,1)S(1)}, u32[]{:S(2)}, u32[]{:S(2)}) collective-permute-start(bf16[192,512]{1,0:T(8,128)(2,1)S(1)} %slice.275), channel_id=1, source_target_pairs={{0,1},{1,0},{2,3},{3,2},{4,5},{5,4},{6,7},{7,6},{8,9},{9,8},{10,11... | collective-permute-start | bytes 589832 | tf_op jit(solution)/shard_map/ppermute | solution.py:18
  118.4 18.5 %collective-permute-start.31 = (bf16[192,512]{1,0:T(8,128)(2,1)S(1)}, bf16[192,512]{1,0:T(8,128)(2,1)S(1)}, u32[]{:S(2)}, u32[]{:S(2)}) collective-permute-start(bf16[192,512]{1,0:T(8,128)(2,1)S(1)} %slice.274), channel_id=1, source_target_pairs={{0,2},{1,3},{2,0},{3,1},{4,6},{5,7},{6,4},{7,5},{8,10},{9,11},{10,... | collective-permute-start | bytes 589832 | tf_op jit(solution)/shard_map/ppermute | solution.py:18
  124.7 22.5 %collective-permute-start.42 = (bf16[384,512]{1,0:T(8,128)(2,1)S(1)}, bf16[384,512]{1,0:T(8,128)(2,1)S(1)}, u32[]{:S(2)}, u32[]{:S(2)}) collective-permute-start(bf16[384,512]{1,0:T(8,128)(2,1)S(1)} %constant_dynamic-update-slice_fusion.8), channel_id=1, source_target_pairs={{0,2},{1,3},{2,0},{3,1},{4,6},{5,7},{6,4},{7,5},{8,10},{9,11},{10,... | collective-permute-start | bytes 1179656 | tf_op jit(solution)/shard_map/ppermute | solution.py:18
  126.2 14.7 %collective-permute-start.23 = (bf16[192,512]{1,0:T(8,128)(2,1)S(1)}, bf16[192,512]{1,0:T(8,128)(2,1)S(1)}, u32[]{:S(2)}, u32[]{:S(2)}) collective-permute-start(bf16[192,512]{1,0:T(8,128)(2,1)S(1)} %slice.269), channel_id=1, source_target_pairs={{0,2},{1,3},{2,0},{3,1},{4,6},{5,7},{6,4},{7,5},{8,10},{9,11},{10,... | collective-permute-start | bytes 589832 | tf_op jit(solution)/shard_map/ppermute | solution.py:18
  136.4 6.0 %collective-permute-start.24 = (bf16[192,512]{1,0:T(8,128)(2,1)S(1)}, bf16[192,512]{1,0:T(8,128)(2,1)S(1)}, u32[]{:S(2)}, u32[]{:S(2)}) collective-permute-start(bf16[192,512]{1,0:T(8,128)(2,1)S(1)} %slice.270), channel_id=1, source_target_pairs={{0,1},{1,0},{2,3},{3,2},{4,5},{5,4},{6,7},{7,6},{8,9},{9,8},{10,11... | collective-permute-start | bytes 589832 | tf_op jit(solution)/shard_map/ppermute | solution.py:18
  143.4 9.7 %collective-permute-start.25 = (bf16[192,512]{1,0:T(8,128)(2,1)S(1)}, bf16[192,512]{1,0:T(8,128)(2,1)S(1)}, u32[]{:S(2)}, u32[]{:S(2)}) collective-permute-start(bf16[192,512]{1,0:T(8,128)(2,1)S(1)} %get-tuple-element.113), channel_id=1, source_target_pairs={{0,24},{4,28},{8,16},{12,20},{16,8},{20,12},{24,0},{28,4},{1,25},{... | collective-permute-start | bytes 589832 | tf_op jit(solution)/shard_map/ppermute | solution.py:18
  144.1 9.1 %collective-permute-start.26 = (bf16[192,512]{1,0:T(8,128)(2,1)S(1)}, bf16[192,512]{1,0:T(8,128)(2,1)S(1)}, u32[]{:S(2)}, u32[]{:S(2)}) collective-permute-start(bf16[192,512]{1,0:T(8,128)(2,1)S(1)} %get-tuple-element.112), channel_id=1, source_target_pairs={{0,28},{4,24},{8,20},{12,16},{16,12},{20,8},{24,4},{28,0},{1,29},{... | collective-permute-start | bytes 589832 | tf_op jit(solution)/shard_map/ppermute | solution.py:18
  145.2 28.4 %collective-permute-start.33 = (bf16[384,512]{1,0:T(8,128)(2,1)S(1)}, bf16[384,512]{1,0:T(8,128)(2,1)S(1)}, u32[]{:S(2)}, u32[]{:S(2)}) collective-permute-start(bf16[384,512]{1,0:T(8,128)(2,1)S(1)} %fusion.159), channel_id=1, source_target_pairs={{0,1},{1,0},{2,3},{3,2},{4,5},{5,4},{6,7},{7,6},{8,9},{9,8},{10,11... | collective-permute-start | bytes 1179656 | tf_op jit(solution)/shard_map/ppermute | solution.py:18
  145.8 27.8 %collective-permute-start.34 = (bf16[384,512]{1,0:T(8,128)(2,1)S(1)}, bf16[384,512]{1,0:T(8,128)(2,1)S(1)}, u32[]{:S(2)}, u32[]{:S(2)}) collective-permute-start(bf16[384,512]{1,0:T(8,128)(2,1)S(1)} %fusion.159), channel_id=1, source_target_pairs={{0,2},{1,3},{2,0},{3,1},{4,6},{5,7},{6,4},{7,5},{8,10},{9,11},{10,... | collective-permute-start | bytes 1179656 | tf_op jit(solution)/shard_map/ppermute | solution.py:18
  147.3 28.9 %collective-permute-start.51 = (bf16[384,512]{1,0:T(8,128)(2,1)S(1)}, bf16[384,512]{1,0:T(8,128)(2,1)S(1)}, u32[]{:S(2)}, u32[]{:S(2)}) collective-permute-start(bf16[384,512]{1,0:T(8,128)(2,1)S(1)} %fusion.157), channel_id=1, source_target_pairs={{0,1},{1,0},{2,3},{3,2},{4,5},{5,4},{6,7},{7,6},{8,9},{9,8},{10,11... | collective-permute-start | bytes 1179656 | tf_op jit(solution)/shard_map/ppermute | solution.py:18
  153.1 15.3 %collective-permute-start.44 = (bf16[192,512]{1,0:T(8,128)(2,1)S(1)}, bf16[192,512]{1,0:T(8,128)(2,1)S(1)}, u32[]{:S(2)}, u32[]{:S(2)}) collective-permute-start(bf16[192,512]{1,0:T(8,128)(2,1)S(1)} %slice.283), channel_id=1, source_target_pairs={{0,1},{1,0},{2,3},{3,2},{4,5},{5,4},{6,7},{7,6},{8,9},{9,8},{10,11... | collective-permute-start | bytes 589832 | tf_op jit(solution)/shard_map/ppermute | solution.py:18
  153.2 17.4 %collective-permute-start.43 = (bf16[192,512]{1,0:T(8,128)(2,1)S(1)}, bf16[192,512]{1,0:T(8,128)(2,1)S(1)}, u32[]{:S(2)}, u32[]{:S(2)}) collective-permute-start(bf16[192,512]{1,0:T(8,128)(2,1)S(1)} %slice.282), channel_id=1, source_target_pairs={{0,2},{1,3},{2,0},{3,1},{4,6},{5,7},{6,4},{7,5},{8,10},{9,11},{10,... | collective-permute-start | bytes 589832 | tf_op jit(solution)/shard_map/ppermute | solution.py:18
  168.4 12.0 %collective-permute-start.52 = (bf16[384,512]{1,0:T(8,128)(2,1)S(1)}, bf16[384,512]{1,0:T(8,128)(2,1)S(1)}, u32[]{:S(2)}, u32[]{:S(2)}) collective-permute-start(bf16[384,512]{1,0:T(8,128)(2,1)S(1)} %fusion.157), channel_id=1, source_target_pairs={{0,2},{1,3},{2,0},{3,1},{4,6},{5,7},{6,4},{7,5},{8,10},{9,11},{10,... | collective-permute-start | bytes 1179656 | tf_op jit(solution)/shard_map/ppermute | solution.py:18
  173.7 10.9 %collective-permute-start.35 = (bf16[192,512]{1,0:T(8,128)(2,1)S(1)}, bf16[192,512]{1,0:T(8,128)(2,1)S(1)}, u32[]{:S(2)}, u32[]{:S(2)}) collective-permute-start(bf16[192,512]{1,0:T(8,128)(2,1)S(1)} %slice.278), channel_id=1, source_target_pairs={{0,2},{1,3},{2,0},{3,1},{4,6},{5,7},{6,4},{7,5},{8,10},{9,11},{10,... | collective-permute-start | bytes 589832 | tf_op jit(solution)/shard_map/ppermute | solution.py:18
  173.8 10.9 %collective-permute-start.36 = (bf16[192,512]{1,0:T(8,128)(2,1)S(1)}, bf16[192,512]{1,0:T(8,128)(2,1)S(1)}, u32[]{:S(2)}, u32[]{:S(2)}) collective-permute-start(bf16[192,512]{1,0:T(8,128)(2,1)S(1)} %slice.279), channel_id=1, source_target_pairs={{0,1},{1,0},{2,3},{3,2},{4,5},{5,4},{6,7},{7,6},{8,9},{9,8},{10,11... | collective-permute-start | bytes 589832 | tf_op jit(solution)/shard_map/ppermute | solution.py:18
  174.6 15.4 %collective-permute-start.45 = (bf16[384,512]{1,0:T(8,128)(2,1)S(1)}, bf16[384,512]{1,0:T(8,128)(2,1)S(1)}, u32[]{:S(2)}, u32[]{:S(2)}) collective-permute-start(bf16[384,512]{1,0:T(8,128)(2,1)S(1)} %fusion.158), channel_id=1, source_target_pairs={{0,1},{1,0},{2,3},{3,2},{4,5},{5,4},{6,7},{7,6},{8,9},{9,8},{10,11... | collective-permute-start | bytes 1179656 | tf_op jit(solution)/shard_map/ppermute | solution.py:18
  176.2 16.9 %collective-permute-start.46 = (bf16[384,512]{1,0:T(8,128)(2,1)S(1)}, bf16[384,512]{1,0:T(8,128)(2,1)S(1)}, u32[]{:S(2)}, u32[]{:S(2)}) collective-permute-start(bf16[384,512]{1,0:T(8,128)(2,1)S(1)} %fusion.158), channel_id=1, source_target_pairs={{0,2},{1,3},{2,0},{3,1},{4,6},{5,7},{6,4},{7,5},{8,10},{9,11},{10,... | collective-permute-start | bytes 1179656 | tf_op jit(solution)/shard_map/ppermute | solution.py:18
  184.6 9.3 %collective-permute-start.54 = (bf16[192,512]{1,0:T(8,128)(2,1)S(1)}, bf16[192,512]{1,0:T(8,128)(2,1)S(1)}, u32[]{:S(2)}, u32[]{:S(2)}) collective-permute-start(bf16[192,512]{1,0:T(8,128)(2,1)S(1)} %slice.293), channel_id=1, source_target_pairs={{0,1},{1,0},{2,3},{3,2},{4,5},{5,4},{6,7},{7,6},{8,9},{9,8},{10,11... | collective-permute-start | bytes 589832 | tf_op jit(solution)/shard_map/ppermute | solution.py:18
  185.4 11.9 %collective-permute-start.53 = (bf16[192,512]{1,0:T(8,128)(2,1)S(1)}, bf16[192,512]{1,0:T(8,128)(2,1)S(1)}, u32[]{:S(2)}, u32[]{:S(2)}) collective-permute-start(bf16[192,512]{1,0:T(8,128)(2,1)S(1)} %slice.292), channel_id=1, source_target_pairs={{0,2},{1,3},{2,0},{3,1},{4,6},{5,7},{6,4},{7,5},{8,10},{9,11},{10,... | collective-permute-start | bytes 589832 | tf_op jit(solution)/shard_map/ppermute | solution.py:18
  187.9 15.1 %collective-permute-start.37 = (bf16[192,512]{1,0:T(8,128)(2,1)S(1)}, bf16[192,512]{1,0:T(8,128)(2,1)S(1)}, u32[]{:S(2)}, u32[]{:S(2)}) collective-permute-start(bf16[192,512]{1,0:T(8,128)(2,1)S(1)} %get-tuple-element.115), channel_id=1, source_target_pairs={{0,16},{4,20},{8,24},{12,28},{16,0},{20,4},{24,8},{28,12},{1,17},{... | collective-permute-start | bytes 589832 | tf_op jit(solution)/shard_map/ppermute | solution.py:18
  190.0 14.5 %collective-permute-start.38 = (bf16[192,512]{1,0:T(8,128)(2,1)S(1)}, bf16[192,512]{1,0:T(8,128)(2,1)S(1)}, u32[]{:S(2)}, u32[]{:S(2)}) collective-permute-start(bf16[192,512]{1,0:T(8,128)(2,1)S(1)} %get-tuple-element.114), channel_id=1, source_target_pairs={{0,20},{4,16},{8,28},{12,24},{16,4},{20,0},{24,12},{28,8},{1,21},{... | collective-permute-start | bytes 589832 | tf_op jit(solution)/shard_map/ppermute | solution.py:18
  193.1 12.5 %collective-permute-start.48 = (bf16[192,512]{1,0:T(8,128)(2,1)S(1)}, bf16[192,512]{1,0:T(8,128)(2,1)S(1)}, u32[]{:S(2)}, u32[]{:S(2)}) collective-permute-start(bf16[192,512]{1,0:T(8,128)(2,1)S(1)} %slice.287), channel_id=1, source_target_pairs={{0,1},{1,0},{2,3},{3,2},{4,5},{5,4},{6,7},{7,6},{8,9},{9,8},{10,11... | collective-permute-start | bytes 589832 | tf_op jit(solution)/shard_map/ppermute | solution.py:18
  193.9 11.7 %collective-permute-start.47 = (bf16[192,512]{1,0:T(8,128)(2,1)S(1)}, bf16[192,512]{1,0:T(8,128)(2,1)S(1)}, u32[]{:S(2)}, u32[]{:S(2)}) collective-permute-start(bf16[192,512]{1,0:T(8,128)(2,1)S(1)} %slice.286), channel_id=1, source_target_pairs={{0,2},{1,3},{2,0},{3,1},{4,6},{5,7},{6,4},{7,5},{8,10},{9,11},{10,... | collective-permute-start | bytes 589832 | tf_op jit(solution)/shard_map/ppermute | solution.py:18
  198.3 10.9 %collective-permute-start.55 = (bf16[192,512]{1,0:T(8,128)(2,1)S(1)}, bf16[192,512]{1,0:T(8,128)(2,1)S(1)}, u32[]{:S(2)}, u32[]{:S(2)}) collective-permute-start(bf16[192,512]{1,0:T(8,128)(2,1)S(1)} %get-tuple-element.121), channel_id=1, source_target_pairs={{0,4},{4,0},{8,12},{12,8},{16,20},{20,16},{24,28},{28,24},{1,5},{5... | collective-permute-start | bytes 589832 | tf_op jit(solution)/shard_map/ppermute | solution.py:18
  206.6 12.1 %copy-start.24 = (s32[384]{0:T(512)S(1)}, s32[384]{0:T(512)}, u32[]{:S(2)}) copy-start(s32[384]{0:T(512)} %iota_add_fusion.1) | copy-start | bytes 4612
  206.7 7.7 %collective-permute-start.49 = (bf16[192,512]{1,0:T(8,128)(2,1)S(1)}, bf16[192,512]{1,0:T(8,128)(2,1)S(1)}, u32[]{:S(2)}, u32[]{:S(2)}) collective-permute-start(bf16[192,512]{1,0:T(8,128)(2,1)S(1)} %get-tuple-element.117), channel_id=1, source_target_pairs={{0,8},{4,12},{8,0},{12,4},{16,24},{20,28},{24,16},{28,20},{1,9},{5... | collective-permute-start | bytes 589832 | tf_op jit(solution)/shard_map/ppermute | solution.py:18
  207.6 11.1 %collective-permute-start.50 = (bf16[192,512]{1,0:T(8,128)(2,1)S(1)}, bf16[192,512]{1,0:T(8,128)(2,1)S(1)}, u32[]{:S(2)}, u32[]{:S(2)}) collective-permute-start(bf16[192,512]{1,0:T(8,128)(2,1)S(1)} %get-tuple-element.116), channel_id=1, source_target_pairs={{0,12},{4,8},{8,4},{12,0},{16,28},{20,24},{24,20},{28,16},{1,13},{... | collective-permute-start | bytes 589832 | tf_op jit(solution)/shard_map/ppermute | solution.py:18
  (24 other events, 94.8 us)
